TPU v7x, 32 devices: a whole 2x2x4 slice. The times are simulated.
32 devices in a mesh: sp: 16 (over z, y, x), tp: 2 (over core).
Axes of the slice: x: 2, y: 2, z: 4, core: 2. Of those that a mesh axis runs over, the one named last changes fastest.
Arguments:
- tokens: bfloat16 [2048, 2048], P('sp'), may hold values from -6 to 6
- norm_gain: float32 [2048], replicated, may hold values from 0.1 to 1.9
- conv_value_weight: bfloat16 [2048, 1024], P('sp', 'tp'), may hold values from -0.125 to 0.125
- conv_gate_weight: bfloat16 [2048, 1024], P('sp', 'tp'), may hold values from -0.125 to 0.125
- conv_kernel: float32 [31, 1024], P(None, 'tp'), may hold values from -10 to 10
- conv_bias: float32 [1024], P('tp'), may hold values from -4 to 4
- channel_gain: float32 [1024], P('tp'), may hold values from 0.1 to 1.9
- query_weight: bfloat16 [2048, 2048], P('sp', 'tp'), may hold values from -0.125 to 0.125
- key_weight: bfloat16 [2048, 2048], P('sp', 'tp'), may hold values from -0.125 to 0.125
- value_weight: bfloat16 [2048, 4096], P('sp', 'tp'), may hold values from -0.125 to 0.125
- gate_weight: bfloat16 [2048, 32], replicated, may hold values from -0.125 to 0.125
- gate_offset: float32 [2, 2, 8, 2048], P(None, None, 'tp', 'sp'), may hold values from -110 to 160, as said below
- start_memory: float32 [2, 8, 512, 256], P(None, 'tp'), may hold values from -0.375 to 0.375
- start_norm: float32 [2, 8, 256], P(None, 'tp'), may hold values from -0.375 to 0.375
- start_level: float32 [2, 8], P(None, 'tp'), may hold values from 2 to 5
- cell_gain: float32 [4096], P('tp'), may hold values from 0.1 to 1.9
- out_conv_weight: bfloat16 [2048, 1024], P('sp', 'tp'), may hold values from -0.25 to 0.25
- out_cell_weight: bfloat16 [2048, 4096], P('sp', 'tp'), may hold values from -0.09375 to 0.09375
Outputs:
- mixed: bfloat16 [2048, 2048], P(('sp', 'tp'))
Inputs may be any that keep to these rules, and one draw needn't show every extreme that they name: `gate_offset`: added to the gate pre-activations; index 0 of the second dimension is the input gate, index 1 the forget gate.
All inputs are finite; a program needn't handle non-finite values.
Results may differ from a plain program's by a relative error of at most 0.017.
Values may be sent and summed in bfloat16 or wider, within the bound.
No kernel may reach another device: no remote copies, remote signals or barrier semaphores. Data moves between devices by JAX's collectives and lax.ppermute only.
A program may use at most 192 MiB of HBM per device.

v0:
```python
import math

import jax
import jax.numpy as jnp
from jax import lax
from jax.experimental import pallas as pl
from jax.experimental.pallas import tpu as pltpu
from jax.sharding import PartitionSpec as P


EPS = 1e-06
LOW = -1e30
F32 = jnp.float32
BF16 = jnp.bfloat16


def dot(a, b, dims=((1,), (0,))):
    return lax.dot_general(a, b, (dims, ((), ())), preferred_element_type=F32)


def pick(stack, index, axis=0):
    return lax.dynamic_index_in_dim(stack, index, axis, keepdims=False)


class Layout:
    def __init__(self, heads_here):
        self.S = lax.axis_size("sp")
        self.T = lax.axis_size("tp")
        self.C = math.gcd(heads_here, self.S)
        self.R = self.S // self.C
        s = lax.axis_index("sp")
        self.h = s // self.R
        self.q = s % self.R
        self.c = lax.axis_index("tp")

    def along_h(self, x, d):
        C, R = self.C, self.R
        return lax.ppermute(
            x, "sp", [(h * R + q, (h + d) % C * R + q) for h in range(C) for q in range(R)]
        )

    def along_q(self, x, d):
        C, R = self.C, self.R
        return lax.ppermute(
            x, "sp", [(h * R + q, h * R + (q + d) % R) for h in range(C) for q in range(R)]
        )

    def flip_q(self, x, d):
        C, R = self.C, self.R
        return lax.ppermute(
            x, "sp", [(h * R + q, h * R + (q ^ d)) for h in range(C) for q in range(R)]
        )

    def along_tp(self, x, d):
        T = self.T
        return lax.ppermute(x, "tp", [(c, (c + d) % T) for c in range(T)])

    def to_part(self, x, d):
        C, R = self.C, self.R
        return lax.ppermute(
            x, "sp", [(s, (s % C + d) % C * R + s // C) for s in range(self.S)]
        )

    def spread_heads(self, chunks_of):
        C = self.C
        got = [chunks_of(self.h)]
        for d in range(1, C):
            got.append(self.along_h(chunks_of((self.h + d) % C), d))
        rev = [got[(-k) % C] for k in range(C)]
        if C == 1:
            return rev[0][None]
        twice = jnp.stack(rev + rev)
        return lax.dynamic_slice_in_dim(twice, (C - self.h) % C, C, 0)

    def gather_parts(self, x):
        R = self.R
        n = x.shape[0]
        if R == 4 and n % 2 == 0:
            a = self.flip_q(x, 1)
            b = self.flip_q(x, 2)
            m = n // 2
            c = self.flip_q(a[:m], 2)
            d = self.flip_q(b[m:], 1)
            return [
                (self.q, 0, n, x),
                (self.q ^ 1, 0, n, a),
                (self.q ^ 2, 0, n, b),
                (self.q ^ 3, 0, m, c),
                (self.q ^ 3, m, n, d),
            ]
        if R <= 8:
            return [(self.q, 0, n, x)] + [
                ((self.q - d) % R, 0, n, self.along_q(x, d)) for d in range(1, R)
            ]
        groups = [[h * R + q for q in range(R)] for h in range(self.C)]
        g = lax.all_gather(x, "sp", axis=0, axis_index_groups=groups, tiled=False)
        return [(q, 0, n, g[q]) for q in range(R)]


def shards_general(
    tokens,
    norm_gain,
    conv_value_weight,
    conv_gate_weight,
    conv_kernel,
    conv_bias,
    channel_gain,
    query_weight,
    key_weight,
    value_weight,
    gate_weight,
    gate_offset,
    start_memory,
    start_norm,
    start_level,
    cell_gain,
    out_conv_weight,
    out_cell_weight,
):
    heads_here = start_level.shape[1]
    L = Layout(heads_here)
    S, T, C, R, h, q, c = L.S, L.T, L.C, L.R, L.h, L.q, L.c
    HL = heads_here // C
    B = tokens.shape[0]
    D = tokens.shape[1]
    N = B * C
    rows = D // S
    key_width = start_norm.shape[2]
    value_width = start_memory.shape[2]
    chan = conv_bias.shape[0] // C
    conv_all = conv_bias.shape[0] * T

    def mine(x, axis):
        n = x.shape[axis] // C
        return lax.dynamic_slice_in_dim(x, h * n, n, axis)

    features = tokens.astype(F32)
    normed = (
        features * lax.rsqrt(jnp.mean(features * features, axis=1, keepdims=True) + EPS) * norm_gain
    ).astype(BF16)
    normed = normed.reshape(B, C, R, rows).transpose(0, 2, 1, 3).reshape(B, D)
    half = D // T
    share = lax.dynamic_slice_in_dim(normed, c * half, half, 1)

    def columns(weights, line):
        return jnp.concatenate(
            [
                lax.dynamic_slice_in_dim(w, line * (w.shape[1] // C), w.shape[1] // C, 1)
                for w in weights
            ],
            axis=1,
        )

    def first(weights):
        got = L.spread_heads(lambda line: columns(weights, line))
        return got.reshape(C * rows, got.shape[2])

    conv_piece = first((conv_value_weight, conv_gate_weight))
    key_piece = first((key_weight,))
    value_piece = first((value_weight,))
    query_piece = first((query_weight,))

    got_tokens = [L.to_part(share, d) if C > 1 else share for d in range(C)]
    offsets = gate_offset.reshape(2, 2, C, HL, B)
    j_here = lax.axis_index("sp") % C
    got_offset = [
        L.to_part(pick(offsets, (j_here + d) % C, 2), d) if C > 1 else offsets[:, :, 0]
        for d in range(C)
    ]

    def in_order(got, axis):
        if C == 1:
            return got[0]
        rev = [got[(-k) % C] for k in range(C)]
        twice = jnp.concatenate(rev + rev, axis=axis)
        n = got[0].shape[axis]
        return lax.dynamic_slice_in_dim(twice, (C - h) % C * n, C * n, axis)

    share_all = in_order(got_tokens, 0)
    offset_all = in_order(got_offset, 3)
    others = [L.along_tp(share_all, d) for d in range(1, T)]
    parts = [share_all] + others
    rev = [parts[(-k) % T] for k in range(T)]
    hidden = lax.dynamic_slice_in_dim(
        jnp.concatenate(rev + rev, axis=1), (T - c) % T * half, D, 1
    )

    wide = C * rows

    def project(piece):
        total = None
        for part, lo, hi, w in L.gather_parts(piece):
            x = lax.dynamic_slice_in_dim(hidden, part * wide + lo, hi - lo, 1)
            y = dot(x, w)
            total = y if total is None else total + y
        return total

    conv_pre = project(conv_piece).astype(BF16)
    keys = project(key_piece).astype(BF16)
    values = project(value_piece).astype(BF16)
    queries = project(query_piece).astype(BF16)

    out_piece = L.spread_heads(
        lambda line: columns((out_conv_weight, out_cell_weight), line)
    ).reshape(C * rows, -1)
    out_rows = jnp.zeros((D, out_piece.shape[1]), BF16)
    for part, lo, hi, w in L.gather_parts(out_piece):
        out_rows = lax.dynamic_update_slice(out_rows, w, (part * wide + lo, 0))

    conv_value = conv_pre[:, :chan].astype(F32)
    conv_gate = conv_pre[:, chan:].astype(F32)
    gated = (conv_value * jax.nn.sigmoid(conv_gate)).astype(BF16)
    reach = conv_kernel.shape[0] // 2
    line_up = [(l * R + i, l * R + i + 1) for l in range(C) for i in range(R - 1)]
    before = lax.ppermute(gated[N - reach :], "sp", line_up)
    after = lax.ppermute(gated[:reach], "sp", [(b, a) for a, b in line_up])
    padded = jnp.concatenate([before, gated, after], axis=0).astype(F32)
    taps = mine(conv_kernel, 1)
    conv_sum = mine(conv_bias, 0) + sum(
        taps[k] * padded[k : k + N] for k in range(taps.shape[0])
    )
    stats = jnp.stack([jnp.sum(conv_sum, axis=1), jnp.sum(conv_sum * conv_sum, axis=1)])
    total = stats
    for d in range(C):
        for e in range(T):
            if d or e:
                total = total + lax.ppermute(
                    stats,
                    ("sp", "tp"),
                    [
                        ((l * R + p) * T + t, ((l + d) % C * R + p) * T + (t + e) % T)
                        for l in range(C)
                        for p in range(R)
                        for t in range(T)
                    ],
                )
    mean = total[0] / conv_all
    var = total[1] / conv_all - mean * mean
    conv_out = jax.nn.silu(
        (conv_sum - mean[:, None]) * lax.rsqrt(var + EPS)[:, None] * mine(channel_gain, 0)
    ).astype(BF16)

    groups = gate_weight.shape[1] // 4
    gates_w = gate_weight.reshape(C, R, rows, 4, groups)
    gates_w = lax.dynamic_slice_in_dim(gates_w, c * heads_here + h * HL, HL, 4)
    gates_w = gates_w.transpose(1, 0, 2, 3, 4).reshape(D, 4 * HL)
    gate_pre = dot(gates_w, hidden, ((0,), (1,))).reshape(2, 2, HL, N) + offset_all
    in_gate = gate_pre[:, 0]
    log_forget = jax.nn.log_sigmoid(gate_pre[:, 1])
    upto = (jnp.arange(N)[:, None] <= jnp.arange(N)[None, :]).astype(F32)
    forward_sum = jnp.dot(log_forget[0], upto, precision=lax.Precision.HIGHEST)
    backward_sum = jnp.dot(log_forget[1], upto.T, precision=lax.Precision.HIGHEST)
    sums = jnp.stack([forward_sum, backward_sum])
    passed = jnp.stack([forward_sum[:, -1], backward_sum[:, 0]])
    tail = passed[:, :, None] - sums + in_gate
    level = jnp.max(tail, axis=2)
    new_weight = jnp.exp(tail - level[:, :, None])
    my_memory = mine(start_memory, 1)
    my_norm = mine(start_norm, 1)
    my_level = mine(start_level, 1)
    step = jnp.arange(N)
    cells = []
    scale = key_width ** (-0.5)
    for i in range(HL):
        k = keys[:, i * key_width : (i + 1) * key_width] * jnp.asarray(scale, BF16)
        v = values[:, i * value_width : (i + 1) * value_width]
        qr = queries[:, i * key_width : (i + 1) * key_width]
        memories = []
        norms = []
        for d in range(2):
            w = new_weight[d, i]
            memories.append(dot((v.astype(F32) * w[:, None]).astype(BF16), k, ((0,), (0,))))
            norms.append(jnp.sum(w[:, None] * k.astype(F32), axis=0))
        memories = jnp.stack(memories).astype(BF16)
        smalls = jnp.concatenate(
            [jnp.stack(norms), level[:, i, None], passed[:, i, None]], axis=1
        )
        if R <= 8:
            got = []
            for d in range(1, R):
                back = jnp.where(q + d < R, 0, 1)
                got.append(
                    (L.along_q(pick(memories, back), d), L.along_q(pick(smalls, back), d))
                )
            get = lambda direction, dist: got[dist - 1 if direction == 0 else R - dist - 1]
        else:
            groups_q = [[l * R + p for p in range(R)] for l in range(C)]
            all_m = lax.all_gather(memories, "sp", axis=0, axis_index_groups=groups_q)
            all_s = lax.all_gather(smalls, "sp", axis=0, axis_index_groups=groups_q)

            def get(direction, dist):
                p = (q - dist) % R if direction == 0 else (q + dist) % R
                return pick(all_m, p)[direction], pick(all_s, p)[direction]

        scores = dot(qr, k, ((1,), (1,)))
        table_sum = None
        carried = None
        for direction in range(2):
            levels, mems, nrms = [], [], []
            decay = jnp.zeros((), F32)
            for dist in range(1, R):
                m, sm = get(direction, dist)
                there = q >= dist if direction == 0 else q + dist < R
                levels.append(jnp.where(there, sm[-2] + decay, LOW))
                mems.append(m)
                nrms.append(sm[:-2])
                decay = decay + jnp.where(there, sm[-1], 0.0)
            levels.append(my_level[direction, i] + decay)
            mems.append(my_memory[direction, i])
            nrms.append(my_norm[direction, i])
            run_level = levels[0]
            for lv in levels[1:]:
                run_level = jnp.maximum(run_level, lv)
            ws = [jnp.exp(lv - run_level) for lv in levels]
            memory = sum(w * m.astype(F32) for w, m in zip(ws, mems)).astype(BF16)
            norm = sum(w * n for w, n in zip(ws, nrms))
            f = sums[direction, i]
            g = in_gate[direction, i]
            mask = step[:, None] >= step[None, :] if direction == 0 else step[:, None] <= step[None, :]
            table = jnp.where(mask, f[:, None] + (g - f)[None, :], -jnp.inf)
            entry = f + run_level
            top = jnp.maximum(jnp.max(table, axis=1), entry)
            weights = scores * jnp.exp(table - top[:, None])
            ew = jnp.exp(entry - top)
            qn = jnp.sum(qr.astype(F32) * norm[None, :], axis=1)
            den = jnp.sum(weights, axis=1) + ew * qn
            inv = 1.0 / jnp.maximum(jnp.abs(den), 1.0)
            scaled = weights * inv[:, None]
            table_sum = scaled if table_sum is None else table_sum + scaled
            part = dot(qr, memory, ((1,), (1,))) * (ew * inv)[:, None]
            carried = part if carried is None else carried + part
        both = dot(table_sum.astype(BF16), v) + carried
        both = both * lax.rsqrt(jnp.mean(both * both, axis=1, keepdims=True) + EPS)
        gain = lax.dynamic_slice_in_dim(mine(cell_gain, 0), i * value_width, value_width, 0)
        cells.append((both * gain).astype(BF16))

    act = jnp.concatenate([conv_out] + cells, axis=1)
    strip = B // T
    act = act.reshape(C, T, strip, act.shape[1])

    def rows_for(t):
        x = pick(act, t, 1).reshape(C * strip, act.shape[3])
        return dot(x, out_rows, ((1,), (1,)))

    arrived = [L.along_tp(rows_for((c + d) % T).astype(BF16), d) for d in range(1, T)]
    own = rows_for(c)
    for a in arrived:
        own = own + a.astype(F32)
    blocks = own.astype(BF16).reshape(C, strip, D)

    if C == 1:
        final = blocks[0].astype(F32)
    elif C == R:
        got = [pick(blocks, q)]
        for d in range(1, R):
            got.append(L.along_q(pick(blocks, (q + d) % R), d))
        rev = [got[(-k) % R] for k in range(R)]
        by_part = jnp.stack(rev)
        final = pick(by_part, (h - q) % R).astype(F32)
        for d in range(1, C):
            final = final + L.along_h(pick(by_part, (h + d - q) % R), d).astype(F32)
    else:
        final = 0.0
        for d in range(C):
            perm = [(l * R + p, p * C + (l + d) % C) for l in range(C) for p in range(R)]
            final = final + lax.ppermute(pick(blocks, (h + d) % C), "sp", perm).astype(F32)
    final = final.astype(BF16).reshape(strip, R, C, rows).transpose(0, 2, 1, 3)
    return final.reshape(strip, D)


HIGHEST = lax.Precision.HIGHEST
NT = ((1,), (1,))
TN = ((0,), (0,))


def kernel(body, outs, pos, *args, scratch=(), limit=24 << 20, alias=None, part=None, far=False):
    specs, arrays = [], []
    for a in args:
        if isinstance(a, tuple) and a[1] is None:
            a = a[0]
            specs.append(pl.BlockSpec(memory_space=pl.ANY))
        elif isinstance(a, tuple):
            a, block, index = a
            specs.append(pl.BlockSpec(block, lambda i, p, index=index: index(p)))
        else:
            specs.append(pl.BlockSpec(a.shape, lambda i, p, k=a.ndim: (0,) * k))
        arrays.append(a)
    shapes = [pltpu.HBM(s, d) if far else jax.ShapeDtypeStruct(s, d) for s, d in outs]
    if part is None:
        part = [s for s, _ in outs]
    whole = [pl.BlockSpec(s, lambda i, p, k=len(s): (0,) * k) for s in part]
    many = len(shapes) > 1
    return pl.pallas_call(
        body,
        out_shape=shapes if many else shapes[0],
        grid_spec=pltpu.PrefetchScalarGridSpec(
            num_scalar_prefetch=1,
            grid=(1,),
            in_specs=specs,
            out_specs=whole if many else whole[0],
            scratch_shapes=scratch,
        ),
        compiler_params=pltpu.CompilerParams(vmem_limit_bytes=limit),
        input_output_aliases=alias or {},
    )(pos, *arrays)


def hbm(x):
    return pltpu.with_memory_space_constraint(x, pltpu.HBM)


def three(x):
    a = x.astype(BF16).astype(F32)
    b = (x - a).astype(BF16).astype(F32)
    return a, b, x - a - b


def turned_body(pos, *refs):
    outs = refs[-4:]
    each = (len(refs) - 4) // 4
    for d, out in enumerate(outs):
        at = 0
        for w in refs[d * each : (d + 1) * each]:
            out[:, at : at + w.shape[1]] = w[...]
            at += w.shape[1]


def straight_body(pos, *refs):
    out = refs[-1]
    for l in range(out.shape[0]):
        at = 0
        for w in refs[:-1]:
            m = w.shape[1] // out.shape[0]
            out[l, :, at : at + m] = w[:, l * m : (l + 1) * m]
            at += m


def stack_body(pos, g0, g1, g2, g3, out):
    for d, g in enumerate((g0, g1, g2, g3)):
        out[lax.rem(pos[0] - d + 4, 4)] = g[...]


def norm_body(pos, tok, gain, off, share):
    C, R = 4, 4
    B, D = tok.shape
    rows = D // (C * R)
    x = tok[...].astype(F32)
    y = x * lax.rsqrt(jnp.mean(x * x, axis=1, keepdims=True) + EPS) * gain[...]
    y = y.astype(BF16)
    halves = []
    for t in range(2):
        halves.append(
            jnp.concatenate(
                [
                    y[:, (hh * R + qq) * rows : (hh * R + qq + 1) * rows]
                    for qq in (2 * t, 2 * t + 1)
                    for hh in range(C)
                ],
                axis=1,
            )
        )
    share[0:B, :] = jnp.where(pos[2] == 0, halves[0], halves[1])
    o = jnp.concatenate([off[k] for k in range(4)], axis=1)
    a, b, c = three(o)
    extra = jnp.concatenate(
        [jnp.concatenate([a, b], axis=1), jnp.concatenate([c, jnp.zeros_like(c)], axis=1)], axis=0
    )
    extra = jnp.concatenate([extra, jnp.zeros_like(extra)], axis=0)
    share[B : B + 16, :] = extra.astype(BF16)


def arrange_body(pos, g0, g1, g2, g3, own, offs):
    h = pos[0]
    B = own.shape[1]
    for d, g in enumerate((g0, g1, g2, g3)):
        j = lax.rem(h - d + 4, 4)
        own[j] = g[0:B, :]
        e = g[B : B + 16, :].astype(F32)
        row = lax.broadcasted_iota(jnp.int32, e.shape, 0)
        ab = jnp.sum(jnp.where(row == h, e, 0.0), axis=0, keepdims=True)
        cc = jnp.sum(jnp.where(row == h + 4, e, 0.0), axis=0, keepdims=True)
        n = ab.shape[1] // 2
        o = ab[:, :n] + ab[:, n:] + cc[:, :n]
        for k in range(4):
            offs[j, k : k + 1, :] = o[:, k * B : (k + 1) * B]


def fill_hidden(pos, own, other, hid):
    c = pos[2]
    n = own.shape[1] // 2
    for i in range(2):
        hid[2 * c + i] = own[:, i * n : (i + 1) * n]
        hid[2 - 2 * c + i] = other[:, i * n : (i + 1) * n]


def projected(pos, hid, pieces):
    q = pos[1]
    y = None
    for i, w in enumerate(pieces):
        t = dot(hid[q ^ i], w[...])
        y = t if y is None else y + t
    return y


def state_body(
    pos, own, other, a0, a1, a2, a3, b0, b1, b2, b3, gw, offs,
    k_out, v_out, g_out, gated, msg, hid, pre_t
):
    h, q, c = pos[0], pos[1], pos[2]
    fill_hidden(pos, own, other, hid)
    R, N, _ = hid.shape
    kw = k_out.shape[1]
    n = gated.shape[1]
    y = projected(pos, hid, (a0, a1, a2, a3))
    k = (y[:, :kw].astype(BF16).astype(F32) * (kw ** (-0.5))).astype(BF16)
    k_out[...] = k
    a = y[:, kw : kw + n].astype(BF16).astype(F32)
    g = y[:, kw + n :].astype(BF16).astype(F32)
    z = (a * jax.nn.sigmoid(g)).astype(BF16)
    gated[...] = z
    edges = jnp.concatenate([z[0:16, :], z[N - 16 :, :]], axis=1)
    rows = gw.shape[1] // 16
    pre = None
    for p in range(R):
        w = jnp.concatenate(
            [gw[:, (l * R + p) * rows : (l * R + p + 1) * rows] for l in range(4)], axis=1
        )
        t = dot(w, hid[p], NT)
        pre = t if pre is None else pre + t
    pre_t[...] = pre
    heads = gw.shape[0] // 4
    at = c * 4 + h
    pre = jnp.concatenate([pre_t[pl.ds(i * heads + at, 1), :] for i in range(4)], axis=0)
    off = jnp.concatenate([offs[j] for j in range(4)], axis=1)
    pre = pre + off
    lf = jnp.minimum(pre, 0.0) - jnp.log1p(jnp.exp(-jnp.abs(pre)))
    lf8 = jnp.concatenate([lf, lf], axis=0)
    ri = lax.broadcasted_iota(jnp.int32, (N, N), 0)
    ci = lax.broadcasted_iota(jnp.int32, (N, N), 1)
    up = jnp.where(ri <= ci, 1.0, 0.0).astype(BF16)
    down = jnp.where(ri >= ci, 1.0, 0.0).astype(BF16)
    f, b = None, None
    for t in three(lf8):
        t = t.astype(BF16)
        f1, b1_ = dot(t, up), dot(t, down)
        f = f1 if f is None else f + f1
        b = b1_ if b is None else b + b1_
    f, b = f[1:2], b[3:4]
    inf, inb = pre[0:1], pre[2:3]
    pf, pb = f[:, N - 1 : N], b[:, 0:1]
    tf, tb = pf - f + inf, pb - b + inb
    lvf, lvb = jnp.max(tf, axis=1, keepdims=True), jnp.max(tb, axis=1, keepdims=True)
    wf, wb = jnp.exp(tf - lvf), jnp.exp(tb - lvb)
    zero = jnp.zeros_like(f)
    g_out[...] = jnp.concatenate([f, b, inf - f, inb - b, zero, zero, zero, zero], axis=0)
    w8 = jnp.concatenate([wf, wb, zero, zero, zero, zero, zero, zero], axis=0)
    wt = w8.T
    nn = None
    for t in three(w8):
        t = dot(t.astype(BF16), k)
        nn = t if nn is None else nn + t
    v = projected(pos, hid, (b0, b1, b2, b3)).astype(BF16)
    v_out[...] = v
    v32 = v.astype(F32)
    mf = dot((v32 * wt[:, 0:1]).astype(BF16), k, TN).astype(BF16)
    mb = dot((v32 * wt[:, 1:2]).astype(BF16), k, TN).astype(BF16)

    def small(n1, lv, ps):
        wide_ = lambda x: jnp.broadcast_to(x, n1.shape)
        r = list(three(n1)) + [wide_(x) for x in three(lv)] + [wide_(x) for x in three(ps)]
        return jnp.concatenate(r + [jnp.zeros((7, n1.shape[1]), F32)], axis=0).astype(BF16)

    sf, sb = small(nn[0:1], lvf, pf), small(nn[1:2], lvb, pb)
    vw = mf.shape[0]
    for p in range(R):
        msg[p, vw + 16 : vw + 32, 0 : 2 * n] = edges

        @pl.when(p > q)
        def _():
            msg[p, 0:vw, :] = mf
            msg[p, vw : vw + 16, :] = sf

        @pl.when(p <= q)
        def _():
            msg[p, 0:vw, :] = mb
            msg[p, vw : vw + 16, :] = sb


def conv_body(pos, gated, msg, taps, bias, conv, stats, pad):
    q = pos[1]
    N, n = gated.shape
    K = taps.shape[0]
    at = msg.shape[1] - 16
    last = msg.shape[0] - 1
    left = msg[jnp.maximum(q - 1, 0), at : at + 16, n : 2 * n].astype(F32)
    right = msg[jnp.minimum(q + 1, last), at : at + 16, 0:n].astype(F32)
    pad[0:16, :] = jnp.where(q > 0, left, 0.0)
    pad[16 : 16 + N, :] = gated[...].astype(F32)
    pad[16 + N : 32 + N, :] = jnp.where(q < last, right, 0.0)
    lo = 16 - K // 2
    step = 64
    for r in range(0, N, step):
        acc = jnp.broadcast_to(bias[...], (step, n))
        for k in range(K):
            acc = acc + taps[k : k + 1, :] * pad[lo + k + r : lo + k + r + step, :]
        conv[r : r + step, :] = acc
    x = conv[...]
    ones = jnp.ones((8, n), F32)
    s1 = lax.dot_general(ones, x, (NT, ((), ())), precision=HIGHEST, preferred_element_type=F32)
    s2 = lax.dot_general(ones, x * x, (NT, ((), ())), precision=HIGHEST, preferred_element_type=F32)
    row = lax.broadcasted_iota(jnp.int32, s1.shape, 0)
    both = jnp.where(row == 0, s1, s2)
    for i in range(stats.shape[0]):
        stats[i] = both


def cell_body(
    pos, own, other, c0, c1, c2, c3, k, v, g, msg, mem0, nrm0, lev0, gain, act, hid, qs
):
    h, q = pos[0], pos[1]
    fill_hidden(pos, own, other, hid)
    qs[...] = projected(pos, hid, (c0, c1, c2, c3)).astype(BF16)
    N = qs.shape[0]
    vw = v.shape[1]
    lv, ps, nr = [], [], []
    for p in range(4):
        e = msg[p, vw : vw + 16, :].astype(F32)
        nr.append(e[0:1] + e[1:2] + e[2:3])
        lv.append((e[3:4] + e[4:5] + e[5:6])[:, 0:1])
        ps.append((e[6:7] + e[7:8] + e[8:9])[:, 0:1])
    mems, nrms, runs = [], [], []
    for d in range(2):
        def ok(p):
            return p < q if d == 0 else p > q

        lvs = []
        for p in range(4):
            between = range(p + 1, 4) if d == 0 else range(0, p)
            x = lv[p]
            for m in between:
                x = x + jnp.where(ok(m), ps[m], 0.0)
            lvs.append(jnp.where(ok(p), x, LOW))
        x = lev0[d : d + 1, :]
        x = jnp.where(lax.broadcasted_iota(jnp.int32, x.shape, 1) == h, x, 0.0)
        x = jnp.sum(x, axis=1, keepdims=True)
        for m in range(4):
            x = x + jnp.where(ok(m), ps[m], 0.0)
        lvs.append(x)
        run = lvs[0]
        for y in lvs[1:]:
            run = jnp.maximum(run, y)
        ws = [jnp.exp(y - run) for y in lvs]
        mm = ws[4] * mem0[d, 0]
        nm = ws[4] * nrm0[d, pl.ds(h, 1), :]
        for p in range(4):
            mm = mm + ws[p] * msg[p, 0:vw, :].astype(F32)
            nm = nm + ws[p] * nr[p]
        mems.append(mm.astype(BF16))
        nrms.append(nm)
        runs.append(run)
    gt = g[...].T
    gn = gain[pl.ds(h, 1), :]
    blk = N // 4
    for j in range(4):
        r0 = j * blk
        qb = qs[r0 : r0 + blk, :]
        q32 = qb.astype(F32)
        scores = dot(qb, k[...], NT)
        ri = lax.broadcasted_iota(jnp.int32, (blk, N), 0) + r0
        ci = lax.broadcasted_iota(jnp.int32, (blk, N), 1)
        total, both = None, None
        for d in range(2):
            fc = gt[r0 : r0 + blk, d : d + 1]
            mask = ri >= ci if d == 0 else ri <= ci
            table = jnp.where(mask, fc + g[2 + d : 3 + d, :], -jnp.inf)
            entry = fc + runs[d]
            top = jnp.maximum(jnp.max(table, axis=1, keepdims=True), entry)
            w = scores * jnp.exp(table - top)
            ew = jnp.exp(entry - top)
            den = jnp.sum(w, axis=1, keepdims=True)
            den = den + ew * jnp.sum(q32 * nrms[d], axis=1, keepdims=True)
            inv = 1.0 / jnp.maximum(jnp.abs(den), 1.0)
            w = w * inv
            total = w if total is None else total + w
            part = dot(qb, mems[d], NT) * (ew * inv)
            both = part if both is None else both + part
        both = both + dot(total.astype(BF16), v[...])
        both = both * lax.rsqrt(jnp.mean(both * both, axis=1, keepdims=True) + EPS) * gn
        act[r0 : r0 + blk, act.shape[1] - vw :] = both.astype(BF16)


def join_body(pos, conv, stats, gain, held, act):
    n = conv.shape[1]
    st = stats[0]
    for i in range(1, stats.shape[0]):
        st = st + stats[i]
    width = n * stats.shape[0]
    mean = st[0:1] / width
    var = st[1:2] / width - mean * mean
    mv = jnp.concatenate([mean, lax.rsqrt(var + EPS)] + [jnp.zeros_like(mean)] * 6, axis=0).T
    x = (conv[...] - mv[:, 0:1]) * mv[:, 1:2] * gain[...]
    act[...] = (x * jax.nn.sigmoid(x)).astype(BF16)


def out_body(pos, act, w0, w1, give, keep):
    c = pos[2]
    half = act.shape[1] // 2

    def rows_of(t):
        at = pl.multiple_of(t * half, half)
        return jnp.concatenate([act[p, pl.ds(at, half), :] for p in range(act.shape[0])], axis=0)

    x, y = rows_of(1 - c), rows_of(c)
    m = w0.shape[0]
    for i, w in enumerate((w0, w1)):
        give[:, i * m : (i + 1) * m] = dot(x, w[...], NT).astype(BF16)
    for i, w in enumerate((w0, w1)):
        keep[:, i * m : (i + 1) * m] = dot(y, w[...], NT)


def add_body(pos, keep, got, *outs):
    n = outs[0].shape[0]
    for d, out in enumerate(outs):
        at = pl.multiple_of(lax.rem(pos[0] + d, len(outs)) * n, n)
        out[...] = (keep[pl.ds(at, n), :] + got[pl.ds(at, n), :].astype(F32)).astype(BF16)


def last_body(pos, *refs):
    out, tiles = refs[-2:]
    q = pos[1]
    each = (len(refs) - 2) // 2
    for y in range(2):
        x = None
        for r in refs[y * each : (y + 1) * each]:
            x = r[...].astype(F32) if x is None else x + r[...].astype(F32)
        rows = x.shape[1] // 8
        for i in range(2):
            for l in range(4):
                at = i * 4 + l
                tiles[l * 4 + (q ^ (2 * y + i))] = x[:, at * rows : (at + 1) * rows]
    out[...] = jnp.concatenate([tiles[i] for i in range(16)], axis=1).astype(BF16)


def shards(
    tokens,
    norm_gain,
    conv_value_weight,
    conv_gate_weight,
    conv_kernel,
    conv_bias,
    channel_gain,
    query_weight,
    key_weight,
    value_weight,
    gate_weight,
    gate_offset,
    start_memory,
    start_norm,
    start_level,
    cell_gain,
    out_conv_weight,
    out_cell_weight,
):
    heads_here = start_level.shape[1]
    L = Layout(heads_here)
    S, T, C, R, h, q, c = L.S, L.T, L.C, L.R, L.h, L.q, L.c
    B, D = tokens.shape
    N = B * C
    rows = D // S
    kw = start_norm.shape[2]
    vw = start_memory.shape[2]
    n = conv_bias.shape[0] // C
    fits = C == R == 4 and T == 2 and heads_here == C and B % 128 == 0 and rows % 128 == 0
    fits = fits and n % 128 == 0 and kw % 128 == 0 and vw % 128 == 0 and conv_kernel.shape[0] <= 31
    fits = fits and 2 * n <= kw
    if not fits:
        return shards_general(
            tokens,
            norm_gain,
            conv_value_weight,
            conv_gate_weight,
            conv_kernel,
            conv_bias,
            channel_gain,
            query_weight,
            key_weight,
            value_weight,
            gate_weight,
            gate_offset,
            start_memory,
            start_norm,
            start_level,
            cell_gain,
            out_conv_weight,
            out_cell_weight,
        )
    pos = jnp.stack([h, q, c, jnp.zeros_like(h)]).astype(jnp.int32)
    lines = [[l * R + p for l in range(C)] for p in range(R)]
    planes = [[l * R + p for p in range(R)] for l in range(C)]

    def swap(x, groups, axes="sp"):
        return lax.all_to_all(x, axes, 0, 0, axis_index_groups=groups, tiled=True)

    def flip(x, d):
        return L.flip_q(x, d)

    def at_col(x):
        m = x.shape[1] // C
        return (hbm(x), (x.shape[0], m), lambda p: (0, p[0]))

    wide = C * rows

    def turned(weights):
        blocks = [
            (hbm(w), (rows, w.shape[1] // C), lambda p, d=d: (0, lax.rem(p[0] + d, C)))
            for d in range(C)
            for w in weights
        ]
        width = sum(w.shape[1] for w in weights) // C
        return kernel(turned_body, [((rows, width), BF16)] * C, pos, *blocks)

    def straight(weights):
        width = sum(w.shape[1] for w in weights) // C
        return kernel(straight_body, [((C, rows, width), BF16)], pos, *map(hbm, weights))

    def cross(turn):
        got = [turn[0]]
        for d in range(1, C):
            got.append(L.along_h(turn[d], d))
        shape = (C, rows, turn[0].shape[1])
        out = kernel(stack_body, [(shape, BF16)], pos, *got)
        return out.reshape(wide, -1)

    z_a = cross(turned((key_weight, conv_value_weight, conv_gate_weight)))
    z_b = swap(straight((value_weight,)), lines).reshape(wide, -1)
    share = kernel(
        norm_body,
        [((B + 16, D // 2), BF16)],
        pos,
        hbm(tokens),
        norm_gain.reshape(1, D),
        gate_offset.reshape(4, heads_here, B),
    )
    got = []
    for d in range(C):
        got.append(L.to_part(share, d))
    z_q = cross(turned((query_weight,)))
    z_o = cross(turned((out_conv_weight, out_cell_weight)))

    a1, a2 = flip(z_a, 1), flip(z_a, 2)
    b1, b2 = flip(z_b, 1), flip(z_b, 2)
    a3 = flip(a1, 2)
    b3 = flip(b2, 1)
    q1, q2 = flip(z_q, 1), flip(z_q, 2)
    q3 = flip(q1, 2)
    o1, o2 = flip(z_o, 1), flip(z_o, 2)
    o3 = flip(o1, 2)

    own, offs = kernel(arrange_body, [((C, B, D // 2), BF16), ((C, 4, B), F32)], pos, *got)
    own = own.reshape(N, D // 2)
    other = L.along_tp(own, 1)
    hid = pltpu.VMEM((R, N, wide), BF16)
    keys, values, gates, gated, msg = kernel(
        state_body,
        [
            ((N, kw), BF16),
            ((N, vw), BF16),
            ((8, N), F32),
            ((N, n), BF16),
            ((R, vw + 32, kw), BF16),
        ],
        pos,
        own,
        other,
        z_a,
        a1,
        a2,
        a3,
        z_b,
        b1,
        b2,
        b3,
        gate_weight.T,
        offs,
        scratch=[hid, pltpu.VMEM((gate_weight.shape[1], N), F32)],
        far=True,
    )
    msg = swap(msg, planes)
    conv, stats = kernel(
        conv_body,
        [((N, n), F32), ((C * T, 8, N), F32)],
        pos,
        hbm(gated),
        msg,
        at_col(conv_kernel),
        at_col(conv_bias.reshape(1, C * n)),
        scratch=[pltpu.VMEM((N + 32, n), F32)],
        far=True,
    )
    stats = swap(
        stats,
        [[(l * R + p) * T + t for l in range(C) for t in range(T)] for p in range(R)],
        ("sp", "tp"),
    )
    act = kernel(
        cell_body,
        [((N, n + vw), BF16)],
        pos,
        own,
        other,
        z_q,
        q1,
        q2,
        q3,
        hbm(keys),
        hbm(values),
        hbm(gates),
        msg,
        (hbm(start_memory), (2, 1, vw, kw), lambda p: (0, p[0], 0, 0)),
        hbm(start_norm),
        hbm(start_level),
        hbm(cell_gain.reshape(C, vw)),
        scratch=[hid, pltpu.VMEM((N, kw), BF16)],
    )
    act = kernel(
        join_body,
        [((N, n + vw), BF16)],
        pos,
        hbm(conv),
        stats,
        at_col(channel_gain.reshape(1, C * n)),
        (act, None),
        alias={4: 0},
        part=[(N, n)],
    )
    act = swap(act.reshape(C, B, n + vw), planes)
    ends = []
    for w0, w1 in ((z_o, o1), (o2, o3)):
        give, keep = kernel(
            out_body, [((N // 2, 2 * wide), BF16), ((N // 2, 2 * wide), F32)], pos, act, w0, w1
        )
        give = L.along_tp(give, 1)
        blocks = kernel(add_body, [((B // T, 2 * wide), BF16)] * C, pos, keep, give)
        ends.append(blocks[0])
        for d in range(1, C):
            ends.append(L.along_h(blocks[d], d))
    return kernel(
        last_body, [((B // T, D), BF16)], pos, *ends, scratch=[pltpu.VMEM((16, B // T, rows), F32)]
    )


def solution(mesh):
    in_specs = (
        P("sp", None),
        P(),
        P("sp", "tp"),
        P("sp", "tp"),
        P(None, "tp"),
        P("tp"),
        P("tp"),
        P("sp", "tp"),
        P("sp", "tp"),
        P("sp", "tp"),
        P(),
        P(None, None, "tp", "sp"),
        P(None, "tp", None, None),
        P(None, "tp", None),
        P(None, "tp"),
        P("tp"),
        P("sp", "tp"),
        P("sp", "tp"),
    )
    out_specs = P(("sp", "tp"), None)
    return jax.shard_map(shards, mesh=mesh, in_specs=in_specs, out_specs=out_specs, check_vma=False)
```

profile of v0, /device:TPU:0, one launch (start us, length us, event | category | flops | bytes accessed | tf_op | source)
XLA Modules:
  0.0 234.9 jit_solution(13898975506749190498)
XLA Ops:
  0.1 2.4 %shard_map.176 = bf16[4,128,512]{2,1,0:T(8,128)(2,1)} custom-call(s32[4]{0:T(128)S(1)} %pad_add_fusion.pos, bf16[128,2048]{1,0:T(8,128)(2,1)} %refs_0_.5), custom_call_target="tpu_custom_call" | custom-call | tf_op jit(solution)/shard_map/pallas_call | solution.py:393
  2.5 6.3 %all-to-all-start = ((bf16[4,128,512]{2,1,0:T(8,128)(2,1)}), bf16[4,128,512]{2,1,0:T(8,128)(2,1)S(1)}, u32[]{:S(2)}, u32[]{:S(2)}) async-start(bf16[4,128,512]{2,1,0:T(8,128)(2,1)} %shard_map.176), calls=%async_computation | async-start | bytes 1048576 | tf_op jit(solution)/shard_map/all_to_all | solution.py:802
  15.1 4.2 %collective-permute-start.1 = (bf16[144,1024]{1,0:T(8,128)(2,1)S(1)}, bf16[144,1024]{1,0:T(8,128)(2,1)S(1)}, u32[]{:S(2)}, u32[]{:S(2)}) collective-permute-start(bf16[144,1024]{1,0:T(8,128)(2,1)S(1)} %shard_map.172), channel_id=1, source_target_pairs={{0,8},{2,16},{4,24},{6,0},{8,10},{10,18},{12,26},{14,2},{16,12},{1... | collective-permute-start | bytes 884744 | tf_op jit(solution)/shard_map/ppermute | solution.py:60
  19.3 3.3 %collective-permute-start.2 = (bf16[144,1024]{1,0:T(8,128)(2,1)S(1)}, bf16[144,1024]{1,0:T(8,128)(2,1)S(1)}, u32[]{:S(2)}, u32[]{:S(2)}) collective-permute-start(bf16[144,1024]{1,0:T(8,128)(2,1)S(1)} %shard_map.172), channel_id=1, source_target_pairs={{0,16},{2,24},{4,0},{6,8},{8,18},{10,26},{12,2},{14,10},{16,20},{1... | collective-permute-start | bytes 884744 | tf_op jit(solution)/shard_map/ppermute | solution.py:60
  25.6 2.5 %collective-permute-start.6 = (bf16[128,512]{1,0:T(8,128)(2,1)S(1)}, bf16[128,512]{1,0:T(8,128)(2,1)S(1)}, u32[]{:S(2)}, u32[]{:S(2)}) collective-permute-start(bf16[128,512]{1,0:T(8,128)(2,1)S(1)} %get-tuple-element.41), channel_id=1, source_target_pairs={{0,16},{2,18},{4,20},{6,22},{8,24},{10,26},{12,28},{14,30},{16,0},... | collective-permute-start | bytes 393224 | tf_op jit(solution)/shard_map/ppermute | solution.py:38
  28.1 30.2 %collective-permute-done.6.g2 = bf16[128,512]{1,0:T(8,128)(2,1)S(1)} collective-permute-done((bf16[128,512]{1,0:T(8,128)(2,1)S(1)}, bf16[128,512]{1,0:T(8,128)(2,1)S(1)}, u32[]{:S(2)}, u32[]{:S(2)}) %collective-permute-start.6) | collective-permute-done | bytes 131104 | tf_op jit(solution)/shard_map/ppermute | solution.py:38
  58.5 4.8 %collective-permute-done.7.g3 = bf16[128,512]{1,0:T(8,128)(2,1)S(1)} collective-permute-done((bf16[128,512]{1,0:T(8,128)(2,1)S(1)}, bf16[128,512]{1,0:T(8,128)(2,1)S(1)}, u32[]{:S(2)}, u32[]{:S(2)}) %collective-permute-start.7) | collective-permute-done | bytes 131104 | tf_op jit(solution)/shard_map/ppermute | solution.py:38
  67.5 7.9 %collective-permute-done.8.a1 = bf16[512,512]{1,0:T(8,128)(2,1)} collective-permute-done((bf16[512,512]{1,0:T(8,128)(2,1)S(1)}, bf16[512,512]{1,0:T(8,128)(2,1)}, u32[]{:S(2)}, u32[]{:S(2)}) %collective-permute-start.8) | collective-permute-done | bytes 524320 | tf_op jit(solution)/shard_map/ppermute | solution.py:50
  77.8 2.4 %collective-permute-done.12.b2 = bf16[512,512]{1,0:T(8,128)(2,1)S(1)} collective-permute-done((bf16[512,512]{1,0:T(8,128)(2,1)S(1)}, bf16[512,512]{1,0:T(8,128)(2,1)S(1)}, u32[]{:S(2)}, u32[]{:S(2)}) %collective-permute-start.12) | collective-permute-done | bytes 524320 | tf_op jit(solution)/shard_map/ppermute | solution.py:50
  81.6 9.9 %collective-permute-done.9.a2 = bf16[512,512]{1,0:T(8,128)(2,1)S(1)} collective-permute-done((bf16[512,512]{1,0:T(8,128)(2,1)S(1)}, bf16[512,512]{1,0:T(8,128)(2,1)S(1)}, u32[]{:S(2)}, u32[]{:S(2)}) %collective-permute-start.9) | collective-permute-done | bytes 524320 | tf_op jit(solution)/shard_map/ppermute | solution.py:50
  91.5 10.7 %collective-permute-done.10.a3 = bf16[512,512]{1,0:T(8,128)(2,1)S(1)} collective-permute-done((bf16[512,512]{1,0:T(8,128)(2,1)}, bf16[512,512]{1,0:T(8,128)(2,1)S(1)}, u32[]{:S(2)}, u32[]{:S(2)}) %collective-permute-start.10) | collective-permute-done | bytes 524320 | tf_op jit(solution)/shard_map/ppermute | solution.py:50
  102.2 7.4 %shard_map.177 = (bf16[512,256]{1,0:T(8,128)(2,1)}, bf16[512,512]{1,0:T(8,128)(2,1)}, f32[8,512]{1,0:T(8,128)}, bf16[512,128]{1,0:T(8,128)(2,1)}, bf16[4,544,256]{2,1,0:T(8,128)(2,1)}) custom-call(s32[4]{0:T(128)S(1)} %pad_add_fusion.pos, bf16[512,1024]{1,0:T(8,128)(2,1)S(1)} %bitcast.15, bf16[512,1024]{1,0:T(8,128)(2,1)S(1)} %collective-permute-done.4.other, ...), custom_call_target="tpu_custom_call" | custom-call | tf_op jit(solution)/shard_map/pallas_call | solution.py:393
  109.6 3.5 %all-to-all-start.1 = ((bf16[4,544,256]{2,1,0:T(8,128)(2,1)}), bf16[4,544,256]{2,1,0:T(8,128)(2,1)S(1)}, u32[]{:S(2)}, u32[]{:S(2)}) async-start(bf16[4,544,256]{2,1,0:T(8,128)(2,1)} %get-tuple-element.45), calls=%async_computation.1 | async-start | bytes 2228224 | tf_op jit(solution)/shard_map/all_to_all | solution.py:802
  115.0 3.6 %collective-permute-start.21 = (bf16[128,640]{1,0:T(8,128)(2,1)S(1)}, bf16[128,640]{1,0:T(8,128)(2,1)S(1)}, u32[]{:S(2)}, u32[]{:S(2)}) collective-permute-start(bf16[128,640]{1,0:T(8,128)(2,1)S(1)} %get-tuple-element.57), channel_id=1, source_target_pairs={{0,16},{2,18},{4,20},{6,22},{8,24},{10,26},{12,28},{14,30},{16,0},... | collective-permute-start | bytes 491528 | tf_op jit(solution)/shard_map/ppermute | solution.py:38
  118.8 5.1 %collective-permute-done.20.g1 = bf16[128,640]{1,0:T(8,128)(2,1)S(1)} collective-permute-done((bf16[128,640]{1,0:T(8,128)(2,1)S(1)}, bf16[128,640]{1,0:T(8,128)(2,1)S(1)}, u32[]{:S(2)}, u32[]{:S(2)}) %collective-permute-start.20) | collective-permute-done | bytes 163872 | tf_op jit(solution)/shard_map/ppermute | solution.py:38
  124.0 5.6 %collective-permute-done.21.g2 = bf16[128,640]{1,0:T(8,128)(2,1)S(1)} collective-permute-done((bf16[128,640]{1,0:T(8,128)(2,1)S(1)}, bf16[128,640]{1,0:T(8,128)(2,1)S(1)}, u32[]{:S(2)}, u32[]{:S(2)}) %collective-permute-start.21) | collective-permute-done | bytes 163872 | tf_op jit(solution)/shard_map/ppermute | solution.py:38
  134.2 4.0 %collective-permute-start.14 = (bf16[128,256]{1,0:T(8,128)(2,1)S(1)}, bf16[128,256]{1,0:T(8,128)(2,1)S(1)}, u32[]{:S(2)}, u32[]{:S(2)}) collective-permute-start(bf16[128,256]{1,0:T(8,128)(2,1)S(1)} %get-tuple-element.49), channel_id=1, source_target_pairs={{0,8},{2,10},{4,12},{6,14},{8,16},{10,18},{12,20},{14,22},{16,24},... | collective-permute-start | bytes 196616 | tf_op jit(solution)/shard_map/ppermute | solution.py:38
  138.3 2.4 %collective-permute-start.16 = (bf16[128,256]{1,0:T(8,128)(2,1)S(1)}, bf16[128,256]{1,0:T(8,128)(2,1)S(1)}, u32[]{:S(2)}, u32[]{:S(2)}) collective-permute-start(bf16[128,256]{1,0:T(8,128)(2,1)S(1)} %get-tuple-element.51), channel_id=1, source_target_pairs={{0,24},{2,26},{4,28},{6,30},{8,0},{10,2},{12,4},{14,6},{16,8},{18,... | collective-permute-start | bytes 196616 | tf_op jit(solution)/shard_map/ppermute | solution.py:38
  140.7 3.8 %collective-permute-done.15.g2 = bf16[128,256]{1,0:T(8,128)(2,1)S(1)} collective-permute-done((bf16[128,256]{1,0:T(8,128)(2,1)S(1)}, bf16[128,256]{1,0:T(8,128)(2,1)S(1)}, u32[]{:S(2)}, u32[]{:S(2)}) %collective-permute-start.15) | collective-permute-done | bytes 65568 | tf_op jit(solution)/shard_map/ppermute | solution.py:38
  147.2 6.3 %collective-permute-done.17.c1 = bf16[512,256]{1,0:T(8,128)(2,1)} collective-permute-done((bf16[512,256]{1,0:T(8,128)(2,1)S(1)}, bf16[512,256]{1,0:T(8,128)(2,1)}, u32[]{:S(2)}, u32[]{:S(2)}) %collective-permute-start.17) | collective-permute-done | bytes 262176 | tf_op jit(solution)/shard_map/ppermute | solution.py:50
  155.2 3.2 %shard_map.178 = (f32[512,128]{1,0:T(8,128)}, f32[8,8,512]{2,1,0:T(8,128)}) custom-call(s32[4]{0:T(128)S(1)} %pad_add_fusion.pos, bf16[512,128]{1,0:T(8,128)(2,1)} %get-tuple-element.44.gated, bf16[4,544,256]{2,1,0:T(8,128)(2,1)S(1)} %all-to-all-done.1.msg, f32[31,512]{1,0:T(8,128)} %taps.1, f32[1,512]{1,0:T(1,128)} %bitcast.29), custom_call_target="tpu_custom_call" | custom-call | tf_op jit(solution)/shard_map/pallas_call | solution.py:393
  158.5 5.3 %all-to-all-start.2 = ((f32[8,8,512]{2,1,0:T(8,128)}), f32[8,8,512]{2,1,0:T(8,128)}, u32[]{:S(2)}, u32[]{:S(2)}) async-start(f32[8,8,512]{2,1,0:T(8,128)} %get-tuple-element.47), calls=%async_computation.2 | async-start | bytes 262144 | tf_op jit(solution)/shard_map/all_to_all | solution.py:802
  166.5 7.3 %shard_map.181.held = bf16[512,640]{1,0:T(8,128)(2,1)} custom-call(s32[4]{0:T(128)S(1)} %pad_add_fusion.pos, bf16[512,1024]{1,0:T(8,128)(2,1)S(1)} %bitcast.16, bf16[512,1024]{1,0:T(8,128)(2,1)S(1)} %collective-permute-done.4.other, bf16[512,256]{1,0:T(8,128)(2,1)S(1)} %bitcast.25, bf16[512,256]{1,0:T(8,128)(2,1)} %collective-permute-done.17.c1, ...), custom_call_target="tpu_custom_call" | custom-call | tf_op jit(solution)/shard_map/pallas_call | solution.py:393
  173.8 2.6 %shard_map.182 = bf16[512,640]{1,0:T(8,128)(2,1)} custom-call(s32[4]{0:T(128)S(1)} %pad_add_fusion.pos, f32[512,128]{1,0:T(8,128)} %get-tuple-element.46.conv, f32[8,8,512]{2,1,0:T(8,128)} %all-to-all-done.2.stats, f32[1,512]{1,0:T(1,128)} %bitcast.30, bf16[512,640]{1,0:T(8,128)(2,1)} %shard_map.181.held), custom_call_target="tpu_custom_call", output_to_operand_aliasing={{}: (4, {})} | custom-call | tf_op jit(solution)/shard_map/pallas_call | solution.py:393
  176.4 3.7 %all-to-all-start.3 = ((bf16[4,128,640]{2,1,0:T(8,128)(2,1)}), bf16[4,128,640]{2,1,0:T(8,128)(2,1)S(1)}, u32[]{:S(2)}, u32[]{:S(2)}) async-start(bf16[4,128,640]{2,1,0:T(8,128)(2,1)} %bitcast.12), calls=%async_computation.3 | async-start | bytes 1310720 | tf_op jit(solution)/shard_map/all_to_all | solution.py:802
  181.7 17.6 %collective-permute-done.29.w1 = bf16[512,640]{1,0:T(8,128)(2,1)} collective-permute-done((bf16[512,640]{1,0:T(8,128)(2,1)}, bf16[512,640]{1,0:T(8,128)(2,1)}, u32[]{:S(2)}, u32[]{:S(2)}) %collective-permute-start.29) | collective-permute-done | bytes 655392 | tf_op jit(solution)/shard_map/ppermute | solution.py:50
  199.3 2.9 %all-to-all-done.3.act = bf16[4,128,640]{2,1,0:T(8,128)(2,1)S(1)} async-done(((bf16[4,128,640]{2,1,0:T(8,128)(2,1)}), bf16[4,128,640]{2,1,0:T(8,128)(2,1)S(1)}, u32[]{:S(2)}, u32[]{:S(2)}) %all-to-all-start.3) | async-done | bytes 655392 | tf_op jit(solution)/shard_map/all_to_all | solution.py:802
  202.2 2.8 %shard_map.187 = (bf16[256,1024]{1,0:T(8,128)(2,1)S(1)}, f32[256,1024]{1,0:T(8,128)S(1)}) custom-call(s32[4]{0:T(128)S(1)} %pad_add_fusion.pos, bf16[4,128,640]{2,1,0:T(8,128)(2,1)S(1)} %all-to-all-done.3.act, bf16[512,640]{1,0:T(8,128)(2,1)} %collective-permute-done.28.w0, bf16[512,640]{1,0:T(8,128)(2,1)} %collective-permute-done.29.w1), custom_call_target="tpu_custom_call" | custom-call | tf_op jit(solution)/shard_map/pallas_call | solution.py:393
  205.2 2.8 %shard_map.185 = (bf16[256,1024]{1,0:T(8,128)(2,1)S(1)}, f32[256,1024]{1,0:T(8,128)S(1)}) custom-call(s32[4]{0:T(128)S(1)} %pad_add_fusion.pos, bf16[4,128,640]{2,1,0:T(8,128)(2,1)S(1)} %all-to-all-done.3.act, bf16[512,640]{1,0:T(8,128)(2,1)} %bitcast.13.w0, bf16[512,640]{1,0:T(8,128)(2,1)} %collective-permute-done.23.w1), custom_call_target="tpu_custom_call" | custom-call | tf_op jit(solution)/shard_map/pallas_call | solution.py:393
  210.9 2.4 %collective-permute-start.32 = (bf16[64,1024]{1,0:T(8,128)(2,1)S(1)}, bf16[64,1024]{1,0:T(8,128)(2,1)S(1)}, u32[]{:S(2)}, u32[]{:S(2)}) collective-permute-start(bf16[64,1024]{1,0:T(8,128)(2,1)S(1)} %get-tuple-element.69), channel_id=1, source_target_pairs={{0,16},{2,18},{4,20},{6,22},{8,24},{10,26},{12,28},{14,30},{16,0},... | collective-permute-start | bytes 393224 | tf_op jit(solution)/shard_map/ppermute | solution.py:38
  219.3 7.8 %collective-permute-done.32.refs_6_ = bf16[64,1024]{1,0:T(8,128)(2,1)S(1)} collective-permute-done((bf16[64,1024]{1,0:T(8,128)(2,1)S(1)}, bf16[64,1024]{1,0:T(8,128)(2,1)S(1)}, u32[]{:S(2)}, u32[]{:S(2)}) %collective-permute-start.32) | collective-permute-done | bytes 131104 | tf_op jit(solution)/shard_map/ppermute | solution.py:38
  227.0 6.5 %collective-permute-done.26.refs_2_ = bf16[64,1024]{1,0:T(8,128)(2,1)S(1)} collective-permute-done((bf16[64,1024]{1,0:T(8,128)(2,1)S(1)}, bf16[64,1024]{1,0:T(8,128)(2,1)S(1)}, u32[]{:S(2)}, u32[]{:S(2)}) %collective-permute-start.26) | collective-permute-done | bytes 131104 | tf_op jit(solution)/shard_map/ppermute | solution.py:38
  (72 shorter events, 43.3 us)
Async XLA Ops:
  2.5 62.9 %all-to-all-start = ((bf16[4,128,512]{2,1,0:T(8,128)(2,1)}), bf16[4,128,512]{2,1,0:T(8,128)(2,1)S(1)}, u32[]{:S(2)}, u32[]{:S(2)}) async-start(bf16[4,128,512]{2,1,0:T(8,128)(2,1)} %shard_map.176), calls=%async_computation | async-start | bytes 1048576 | tf_op jit(solution)/shard_map/all_to_all | solution.py:802
  10.5 15.1 %collective-permute-start.5 = (bf16[128,512]{1,0:T(8,128)(2,1)S(1)}, bf16[128,512]{1,0:T(8,128)(2,1)S(1)}, u32[]{:S(2)}, u32[]{:S(2)}) collective-permute-start(bf16[128,512]{1,0:T(8,128)(2,1)S(1)} %get-tuple-element.40), channel_id=1, source_target_pairs={{0,8},{2,10},{4,12},{6,14},{8,16},{10,18},{12,20},{14,22},{16,24},... | collective-permute-start | bytes 393224 | tf_op jit(solution)/shard_map/ppermute | solution.py:38
  14.4 50.2 %collective-permute-start = (bf16[144,1024]{1,0:T(8,128)(2,1)S(1)}, bf16[144,1024]{1,0:T(8,128)(2,1)S(1)}, u32[]{:S(2)}, u32[]{:S(2)}) collective-permute-start(bf16[144,1024]{1,0:T(8,128)(2,1)S(1)} %shard_map.172), channel_id=1, source_target_pairs={{0,0},{2,8},{4,16},{6,24},{8,2},{10,10},{12,18},{14,26},{16,4},{18... | collective-permute-start | bytes 884744 | tf_op jit(solution)/shard_map/ppermute | solution.py:60
  15.1 49.6 %collective-permute-start.1 = (bf16[144,1024]{1,0:T(8,128)(2,1)S(1)}, bf16[144,1024]{1,0:T(8,128)(2,1)S(1)}, u32[]{:S(2)}, u32[]{:S(2)}) collective-permute-start(bf16[144,1024]{1,0:T(8,128)(2,1)S(1)} %shard_map.172), channel_id=1, source_target_pairs={{0,8},{2,16},{4,24},{6,0},{8,10},{10,18},{12,26},{14,2},{16,12},{1... | collective-permute-start | bytes 884744 | tf_op jit(solution)/shard_map/ppermute | solution.py:60
  19.3 45.3 %collective-permute-start.2 = (bf16[144,1024]{1,0:T(8,128)(2,1)S(1)}, bf16[144,1024]{1,0:T(8,128)(2,1)S(1)}, u32[]{:S(2)}, u32[]{:S(2)}) collective-permute-start(bf16[144,1024]{1,0:T(8,128)(2,1)S(1)} %shard_map.172), channel_id=1, source_target_pairs={{0,16},{2,24},{4,0},{6,8},{8,18},{10,26},{12,2},{14,10},{16,20},{1... | collective-permute-start | bytes 884744 | tf_op jit(solution)/shard_map/ppermute | solution.py:60
  22.6 42.1 %collective-permute-start.3 = (bf16[144,1024]{1,0:T(8,128)(2,1)S(1)}, bf16[144,1024]{1,0:T(8,128)(2,1)S(1)}, u32[]{:S(2)}, u32[]{:S(2)}) collective-permute-start(bf16[144,1024]{1,0:T(8,128)(2,1)S(1)} %shard_map.172), channel_id=1, source_target_pairs={{0,24},{2,0},{4,8},{6,16},{8,26},{10,2},{12,10},{14,18},{16,28},{1... | collective-permute-start | bytes 884744 | tf_op jit(solution)/shard_map/ppermute | solution.py:60
  25.6 32.7 %collective-permute-start.6 = (bf16[128,512]{1,0:T(8,128)(2,1)S(1)}, bf16[128,512]{1,0:T(8,128)(2,1)S(1)}, u32[]{:S(2)}, u32[]{:S(2)}) collective-permute-start(bf16[128,512]{1,0:T(8,128)(2,1)S(1)} %get-tuple-element.41), channel_id=1, source_target_pairs={{0,16},{2,18},{4,20},{6,22},{8,24},{10,26},{12,28},{14,30},{16,0},... | collective-permute-start | bytes 393224 | tf_op jit(solution)/shard_map/ppermute | solution.py:38
  63.9 11.5 %collective-permute-start.8 = (bf16[512,512]{1,0:T(8,128)(2,1)S(1)}, bf16[512,512]{1,0:T(8,128)(2,1)}, u32[]{:S(2)}, u32[]{:S(2)}) collective-permute-start(bf16[512,512]{1,0:T(8,128)(2,1)S(1)} %bitcast.20), channel_id=1, source_target_pairs={{0,2},{2,0},{4,6},{6,4},{8,10},{10,8},{12,14},{14,12},{16,18},{18,... | collective-permute-start | bytes 1572872 | tf_op jit(solution)/shard_map/ppermute | solution.py:50
  65.3 36.9 %collective-permute-start.4 = (bf16[512,1024]{1,0:T(8,128)(2,1)S(1)}, bf16[512,1024]{1,0:T(8,128)(2,1)S(1)}, u32[]{:S(2)}, u32[]{:S(2)}) collective-permute-start(bf16[512,1024]{1,0:T(8,128)(2,1)S(1)} %bitcast.14), channel_id=1, source_target_pairs={{0,1},{1,0},{2,3},{3,2},{4,5},{5,4},{6,7},{7,6},{8,9},{9,8},{10,11... | collective-permute-start | bytes 3145736 | tf_op jit(solution)/shard_map/ppermute | solution.py:56
  65.4 14.9 %collective-permute-start.12 = (bf16[512,512]{1,0:T(8,128)(2,1)S(1)}, bf16[512,512]{1,0:T(8,128)(2,1)S(1)}, u32[]{:S(2)}, u32[]{:S(2)}) collective-permute-start(bf16[512,512]{1,0:T(8,128)(2,1)S(1)} %bitcast.17), channel_id=1, source_target_pairs={{0,4},{2,6},{4,0},{6,2},{8,12},{10,14},{12,8},{14,10},{16,20},{18,... | collective-permute-start | bytes 1572872 | tf_op jit(solution)/shard_map/ppermute | solution.py:50
  66.6 24.9 %collective-permute-start.9 = (bf16[512,512]{1,0:T(8,128)(2,1)S(1)}, bf16[512,512]{1,0:T(8,128)(2,1)S(1)}, u32[]{:S(2)}, u32[]{:S(2)}) collective-permute-start(bf16[512,512]{1,0:T(8,128)(2,1)S(1)} %bitcast.21), channel_id=1, source_target_pairs={{0,4},{2,6},{4,0},{6,2},{8,12},{10,14},{12,8},{14,10},{16,20},{18,... | collective-permute-start | bytes 1572872 | tf_op jit(solution)/shard_map/ppermute | solution.py:50
  75.4 26.8 %collective-permute-start.10 = (bf16[512,512]{1,0:T(8,128)(2,1)}, bf16[512,512]{1,0:T(8,128)(2,1)S(1)}, u32[]{:S(2)}, u32[]{:S(2)}) collective-permute-start(bf16[512,512]{1,0:T(8,128)(2,1)} %collective-permute-done.8.a1), channel_id=1, source_target_pairs={{0,4},{2,6},{4,0},{6,2},{8,12},{10,14},{12,8},{14,10},{16,20},{18,... | collective-permute-start | bytes 1572872 | tf_op jit(solution)/shard_map/ppermute | solution.py:50
  76.1 26.1 %collective-permute-start.11 = (bf16[512,512]{1,0:T(8,128)(2,1)S(1)}, bf16[512,512]{1,0:T(8,128)(2,1)S(1)}, u32[]{:S(2)}, u32[]{:S(2)}) collective-permute-start(bf16[512,512]{1,0:T(8,128)(2,1)S(1)} %bitcast.18), channel_id=1, source_target_pairs={{0,2},{2,0},{4,6},{6,4},{8,10},{10,8},{12,14},{14,12},{16,18},{18,... | collective-permute-start | bytes 1572872 | tf_op jit(solution)/shard_map/ppermute | solution.py:50
  80.3 21.9 %collective-permute-start.13 = (bf16[512,512]{1,0:T(8,128)(2,1)S(1)}, bf16[512,512]{1,0:T(8,128)(2,1)S(1)}, u32[]{:S(2)}, u32[]{:S(2)}) collective-permute-start(bf16[512,512]{1,0:T(8,128)(2,1)S(1)} %collective-permute-done.12.b2), channel_id=1, source_target_pairs={{0,2},{2,0},{4,6},{6,4},{8,10},{10,8},{12,14},{14,12},{16,18},{18,... | collective-permute-start | bytes 1572872 | tf_op jit(solution)/shard_map/ppermute | solution.py:50
  109.6 45.6 %all-to-all-start.1 = ((bf16[4,544,256]{2,1,0:T(8,128)(2,1)}), bf16[4,544,256]{2,1,0:T(8,128)(2,1)S(1)}, u32[]{:S(2)}, u32[]{:S(2)}) async-start(bf16[4,544,256]{2,1,0:T(8,128)(2,1)} %get-tuple-element.45), calls=%async_computation.1 | async-start | bytes 2228224 | tf_op jit(solution)/shard_map/all_to_all | solution.py:802
  114.9 9.0 %collective-permute-start.20 = (bf16[128,640]{1,0:T(8,128)(2,1)S(1)}, bf16[128,640]{1,0:T(8,128)(2,1)S(1)}, u32[]{:S(2)}, u32[]{:S(2)}) collective-permute-start(bf16[128,640]{1,0:T(8,128)(2,1)S(1)} %get-tuple-element.56), channel_id=1, source_target_pairs={{0,8},{2,10},{4,12},{6,14},{8,16},{10,18},{12,20},{14,22},{16,24},... | collective-permute-start | bytes 491528 | tf_op jit(solution)/shard_map/ppermute | solution.py:38
  115.0 14.6 %collective-permute-start.21 = (bf16[128,640]{1,0:T(8,128)(2,1)S(1)}, bf16[128,640]{1,0:T(8,128)(2,1)S(1)}, u32[]{:S(2)}, u32[]{:S(2)}) collective-permute-start(bf16[128,640]{1,0:T(8,128)(2,1)S(1)} %get-tuple-element.57), channel_id=1, source_target_pairs={{0,16},{2,18},{4,20},{6,22},{8,24},{10,26},{12,28},{14,30},{16,0},... | collective-permute-start | bytes 491528 | tf_op jit(solution)/shard_map/ppermute | solution.py:38
  118.6 11.0 %collective-permute-start.22 = (bf16[128,640]{1,0:T(8,128)(2,1)S(1)}, bf16[128,640]{1,0:T(8,128)(2,1)S(1)}, u32[]{:S(2)}, u32[]{:S(2)}) collective-permute-start(bf16[128,640]{1,0:T(8,128)(2,1)S(1)} %get-tuple-element.58), channel_id=1, source_target_pairs={{0,24},{2,26},{4,28},{6,30},{8,0},{10,2},{12,4},{14,6},{16,8},{18,... | collective-permute-start | bytes 491528 | tf_op jit(solution)/shard_map/ppermute | solution.py:38
  131.0 33.1 %collective-permute-start.23 = (bf16[512,640]{1,0:T(8,128)(2,1)}, bf16[512,640]{1,0:T(8,128)(2,1)}, u32[]{:S(2)}, u32[]{:S(2)}) collective-permute-start(bf16[512,640]{1,0:T(8,128)(2,1)} %bitcast.13.w0), channel_id=1, source_target_pairs={{0,2},{2,0},{4,6},{6,4},{8,10},{10,8},{12,14},{14,12},{16,18},{18,... | collective-permute-start | bytes 1966088 | tf_op jit(solution)/shard_map/ppermute | solution.py:50
  145.1 8.4 %collective-permute-start.17 = (bf16[512,256]{1,0:T(8,128)(2,1)S(1)}, bf16[512,256]{1,0:T(8,128)(2,1)}, u32[]{:S(2)}, u32[]{:S(2)}) collective-permute-start(bf16[512,256]{1,0:T(8,128)(2,1)S(1)} %bitcast.23), channel_id=1, source_target_pairs={{0,2},{2,0},{4,6},{6,4},{8,10},{10,8},{12,14},{14,12},{16,18},{18,... | collective-permute-start | bytes 786440 | tf_op jit(solution)/shard_map/ppermute | solution.py:50
  145.5 21.0 %collective-permute-start.18 = (bf16[512,256]{1,0:T(8,128)(2,1)S(1)}, bf16[512,256]{1,0:T(8,128)(2,1)}, u32[]{:S(2)}, u32[]{:S(2)}) collective-permute-start(bf16[512,256]{1,0:T(8,128)(2,1)S(1)} %bitcast.24), channel_id=1, source_target_pairs={{0,4},{2,6},{4,0},{6,2},{8,12},{10,14},{12,8},{14,10},{16,20},{18,... | collective-permute-start | bytes 786440 | tf_op jit(solution)/shard_map/ppermute | solution.py:50
  153.5 12.9 %collective-permute-start.19 = (bf16[512,256]{1,0:T(8,128)(2,1)}, bf16[512,256]{1,0:T(8,128)(2,1)}, u32[]{:S(2)}, u32[]{:S(2)}) collective-permute-start(bf16[512,256]{1,0:T(8,128)(2,1)} %collective-permute-done.17.c1), channel_id=1, source_target_pairs={{0,4},{2,6},{4,0},{6,2},{8,12},{10,14},{12,8},{14,10},{16,20},{18,... | collective-permute-start | bytes 786440 | tf_op jit(solution)/shard_map/ppermute | solution.py:50
  158.5 15.3 %all-to-all-start.2 = ((f32[8,8,512]{2,1,0:T(8,128)}), f32[8,8,512]{2,1,0:T(8,128)}, u32[]{:S(2)}, u32[]{:S(2)}) async-start(f32[8,8,512]{2,1,0:T(8,128)} %get-tuple-element.47), calls=%async_computation.2 | async-start | bytes 262144 | tf_op jit(solution)/shard_map/all_to_all | solution.py:802
  163.8 17.9 %collective-permute-start.28 = (bf16[512,640]{1,0:T(8,128)(2,1)}, bf16[512,640]{1,0:T(8,128)(2,1)}, u32[]{:S(2)}, u32[]{:S(2)}) collective-permute-start(bf16[512,640]{1,0:T(8,128)(2,1)} %bitcast.13.w0), channel_id=1, source_target_pairs={{0,4},{2,6},{4,0},{6,2},{8,12},{10,14},{12,8},{14,10},{16,20},{18,... | collective-permute-start | bytes 1966088 | tf_op jit(solution)/shard_map/ppermute | solution.py:50
  164.2 35.1 %collective-permute-start.29 = (bf16[512,640]{1,0:T(8,128)(2,1)}, bf16[512,640]{1,0:T(8,128)(2,1)}, u32[]{:S(2)}, u32[]{:S(2)}) collective-permute-start(bf16[512,640]{1,0:T(8,128)(2,1)} %collective-permute-done.23.w1), channel_id=1, source_target_pairs={{0,4},{2,6},{4,0},{6,2},{8,12},{10,14},{12,8},{14,10},{16,20},{18,... | collective-permute-start | bytes 1966088 | tf_op jit(solution)/shard_map/ppermute | solution.py:50
  176.4 25.9 %all-to-all-start.3 = ((bf16[4,128,640]{2,1,0:T(8,128)(2,1)}), bf16[4,128,640]{2,1,0:T(8,128)(2,1)S(1)}, u32[]{:S(2)}, u32[]{:S(2)}) async-start(bf16[4,128,640]{2,1,0:T(8,128)(2,1)} %bitcast.12), calls=%async_computation.3 | async-start | bytes 1310720 | tf_op jit(solution)/shard_map/all_to_all | solution.py:802
  209.2 8.3 %collective-permute-start.31 = (bf16[64,1024]{1,0:T(8,128)(2,1)S(1)}, bf16[64,1024]{1,0:T(8,128)(2,1)S(1)}, u32[]{:S(2)}, u32[]{:S(2)}) collective-permute-start(bf16[64,1024]{1,0:T(8,128)(2,1)S(1)} %get-tuple-element.68), channel_id=1, source_target_pairs={{0,8},{2,10},{4,12},{6,14},{8,16},{10,18},{12,20},{14,22},{16,24},... | collective-permute-start | bytes 393224 | tf_op jit(solution)/shard_map/ppermute | solution.py:38
  210.9 16.1 %collective-permute-start.32 = (bf16[64,1024]{1,0:T(8,128)(2,1)S(1)}, bf16[64,1024]{1,0:T(8,128)(2,1)S(1)}, u32[]{:S(2)}, u32[]{:S(2)}) collective-permute-start(bf16[64,1024]{1,0:T(8,128)(2,1)S(1)} %get-tuple-element.69), channel_id=1, source_target_pairs={{0,16},{2,18},{4,20},{6,22},{8,24},{10,26},{12,28},{14,30},{16,0},... | collective-permute-start | bytes 393224 | tf_op jit(solution)/shard_map/ppermute | solution.py:38
  213.3 13.7 %collective-permute-start.33 = (bf16[64,1024]{1,0:T(8,128)(2,1)S(1)}, bf16[64,1024]{1,0:T(8,128)(2,1)S(1)}, u32[]{:S(2)}, u32[]{:S(2)}) collective-permute-start(bf16[64,1024]{1,0:T(8,128)(2,1)S(1)} %get-tuple-element.70), channel_id=1, source_target_pairs={{0,24},{2,26},{4,28},{6,30},{8,0},{10,2},{12,4},{14,6},{16,8},{18,... | collective-permute-start | bytes 393224 | tf_op jit(solution)/shard_map/ppermute | solution.py:38
  215.4 11.6 %collective-permute-start.25 = (bf16[64,1024]{1,0:T(8,128)(2,1)S(1)}, bf16[64,1024]{1,0:T(8,128)(2,1)S(1)}, u32[]{:S(2)}, u32[]{:S(2)}) collective-permute-start(bf16[64,1024]{1,0:T(8,128)(2,1)S(1)} %get-tuple-element.62), channel_id=1, source_target_pairs={{0,8},{2,10},{4,12},{6,14},{8,16},{10,18},{12,20},{14,22},{16,24},... | collective-permute-start | bytes 393224 | tf_op jit(solution)/shard_map/ppermute | solution.py:38
  216.0 17.5 %collective-permute-start.26 = (bf16[64,1024]{1,0:T(8,128)(2,1)S(1)}, bf16[64,1024]{1,0:T(8,128)(2,1)S(1)}, u32[]{:S(2)}, u32[]{:S(2)}) collective-permute-start(bf16[64,1024]{1,0:T(8,128)(2,1)S(1)} %get-tuple-element.63), channel_id=1, source_target_pairs={{0,16},{2,18},{4,20},{6,22},{8,24},{10,26},{12,28},{14,30},{16,0},... | collective-permute-start | bytes 393224 | tf_op jit(solution)/shard_map/ppermute | solution.py:38
  217.5 15.9 %collective-permute-start.27 = (bf16[64,1024]{1,0:T(8,128)(2,1)S(1)}, bf16[64,1024]{1,0:T(8,128)(2,1)S(1)}, u32[]{:S(2)}, u32[]{:S(2)}) collective-permute-start(bf16[64,1024]{1,0:T(8,128)(2,1)S(1)} %get-tuple-element.64), channel_id=1, source_target_pairs={{0,24},{2,26},{4,28},{6,30},{8,0},{10,2},{12,4},{14,6},{16,8},{18,... | collective-permute-start | bytes 393224 | tf_op jit(solution)/shard_map/ppermute | solution.py:38
  (10 other events, 112.1 us)
where the time goes:
time: 236 us; the launch traced here: 235 us
  waiting for transfers between devices  125 us (53%)
  starting transfers between devices  67.7 us (29%)
  Pallas kernels  41.3 us (18%)
    ppermute x15, waiting for transfers between devices, along_h(): lax.ppermute(x, 'sp', [(h * R + q, (h + d) % C * R + q) for h in range(C)...  65.5 us
    ppermute x12, waiting for transfers between devices, flip_q(): lax.ppermute(x, 'sp', [(h * R + q, h * R + (q ^ d)) for h in range(C) for...  56.5 us
    pallas_call x18, Pallas kernels, kernel(): pl.pallas_call(body, out_shape=shapes if many else shapes[0], grid_spec=p...  41.3 us
    ppermute x15, starting transfers between devices, along_h(): lax.ppermute(x, 'sp', [(h * R + q, (h + d) % C * R + q) for h in range(C)...  23.5 us
    all_to_all x4, starting transfers between devices, swap(): return lax.all_to_all(x, axes, 0, 0, axis_index_groups=groups, tiled=True)  18.9 us
    ppermute x12, starting transfers between devices, flip_q(): lax.ppermute(x, 'sp', [(h * R + q, h * R + (q ^ d)) for h in range(C) for...  14.2 us
    ppermute x4, starting transfers between devices, to_part(): lax.ppermute(x, 'sp', [(s, (s % C + d) % C * R + s // C) for s in range(s...  10.5 us
  transfers between devices with their start and end apart: 38, of which 17 were waited for; matrix products, arithmetic and copies ran while one was open for 0% of the time, Pallas kernels for 12%

commit v1 on v0

--- a/solution.py
+++ b/solution.py
@@ -504,7 +504,7 @@
 
 def state_body(
     pos, own, other, a0, a1, a2, a3, b0, b1, b2, b3, gw, offs,
-    k_out, v_out, g_out, gated, msg, hid, pre_t
+    k_out, v_out, g_out, gated, head, tail, m1, m2, m3, hid, pre_t
 ):
     h, q, c = pos[0], pos[1], pos[2]
     fill_hidden(pos, own, other, hid)
@@ -518,7 +518,8 @@
     g = y[:, kw + n :].astype(BF16).astype(F32)
     z = (a * jax.nn.sigmoid(g)).astype(BF16)
     gated[...] = z
-    edges = jnp.concatenate([z[0:16, :], z[N - 16 :, :]], axis=1)
+    head[...] = z[0:16, :]
+    tail[...] = z[N - 16 :, :]
     rows = gw.shape[1] // 16
     pre = None
     for p in range(R):
@@ -572,31 +573,24 @@
 
     sf, sb = small(nn[0:1], lvf, pf), small(nn[1:2], lvb, pb)
     vw = mf.shape[0]
-    for p in range(R):
-        msg[p, vw + 16 : vw + 32, 0 : 2 * n] = edges
-
-        @pl.when(p > q)
+    for d, msg in enumerate((m1, m2, m3)):
+        @pl.when(q + d + 1 < R)
         def _():
-            msg[p, 0:vw, :] = mf
-            msg[p, vw : vw + 16, :] = sf
-
-        @pl.when(p <= q)
+            msg[0:vw, :] = mf
+            msg[vw:, :] = sf
+
+        @pl.when(q + d + 1 >= R)
         def _():
-            msg[p, 0:vw, :] = mb
-            msg[p, vw : vw + 16, :] = sb
-
-
-def conv_body(pos, gated, msg, taps, bias, conv, stats, pad):
-    q = pos[1]
+            msg[0:vw, :] = mb
+            msg[vw:, :] = sb
+
+
+def conv_body(pos, gated, before, after, taps, bias, conv, stats, pad):
     N, n = gated.shape
     K = taps.shape[0]
-    at = msg.shape[1] - 16
-    last = msg.shape[0] - 1
-    left = msg[jnp.maximum(q - 1, 0), at : at + 16, n : 2 * n].astype(F32)
-    right = msg[jnp.minimum(q + 1, last), at : at + 16, 0:n].astype(F32)
-    pad[0:16, :] = jnp.where(q > 0, left, 0.0)
+    pad[0:16, :] = before[...].astype(F32)
     pad[16 : 16 + N, :] = gated[...].astype(F32)
-    pad[16 + N : 32 + N, :] = jnp.where(q < last, right, 0.0)
+    pad[16 + N : 32 + N, :] = after[...].astype(F32)
     lo = 16 - K // 2
     step = 64
     for r in range(0, N, step):
@@ -614,52 +608,67 @@
         stats[i] = both
 
 
+def query_body(pos, own, other, c0, c1, c2, c3, qs, hid):
+    fill_hidden(pos, own, other, hid)
+    qs[...] = projected(pos, hid, (c0, c1, c2, c3)).astype(BF16)
+
+
 def cell_body(
-    pos, own, other, c0, c1, c2, c3, k, v, g, msg, mem0, nrm0, lev0, gain, act, hid, qs
+    pos, qs, k, v, g, m1, m2, m3, mem0, nrm0, lev0, gain, conv, stats, chgain, act, past
 ):
     h, q = pos[0], pos[1]
-    fill_hidden(pos, own, other, hid)
-    qs[...] = projected(pos, hid, (c0, c1, c2, c3)).astype(BF16)
-    N = qs.shape[0]
+    N, _ = qs.shape
     vw = v.shape[1]
+    got = (m1, m2, m3)
     lv, ps, nr = [], [], []
-    for p in range(4):
-        e = msg[p, vw : vw + 16, :].astype(F32)
+    for m in got:
+        e = m[vw : vw + 16, :].astype(F32)
         nr.append(e[0:1] + e[1:2] + e[2:3])
         lv.append((e[3:4] + e[4:5] + e[5:6])[:, 0:1])
         ps.append((e[6:7] + e[7:8] + e[8:9])[:, 0:1])
     mems, nrms, runs = [], [], []
     for d in range(2):
-        def ok(p):
-            return p < q if d == 0 else p > q
+        def ok(i):
+            return q >= i + 1 if d == 0 else q < i + 1
 
         lvs = []
-        for p in range(4):
-            between = range(p + 1, 4) if d == 0 else range(0, p)
-            x = lv[p]
+        for i in range(3):
+            between = range(0, i) if d == 0 else range(i + 1, 3)
+            x = lv[i]
             for m in between:
                 x = x + jnp.where(ok(m), ps[m], 0.0)
-            lvs.append(jnp.where(ok(p), x, LOW))
+            lvs.append(jnp.where(ok(i), x, LOW))
         x = lev0[d : d + 1, :]
         x = jnp.where(lax.broadcasted_iota(jnp.int32, x.shape, 1) == h, x, 0.0)
         x = jnp.sum(x, axis=1, keepdims=True)
-        for m in range(4):
+        for m in range(3):
             x = x + jnp.where(ok(m), ps[m], 0.0)
         lvs.append(x)
         run = lvs[0]
         for y in lvs[1:]:
             run = jnp.maximum(run, y)
         ws = [jnp.exp(y - run) for y in lvs]
-        mm = ws[4] * mem0[d, 0]
-        nm = ws[4] * nrm0[d, pl.ds(h, 1), :]
-        for p in range(4):
-            mm = mm + ws[p] * msg[p, 0:vw, :].astype(F32)
-            nm = nm + ws[p] * nr[p]
+        mm = ws[3] * mem0[d, 0]
+        nm = ws[3] * nrm0[d, pl.ds(h, 1), :]
+        for i in range(3):
+            mm = mm + ws[i] * got[i][0:vw, :].astype(F32)
+            nm = nm + ws[i] * nr[i]
         mems.append(mm.astype(BF16))
         nrms.append(nm)
         runs.append(run)
-    gt = g[...].T
-    gn = gain[pl.ds(h, 1), :]
+    for d in range(2):
+        past[d] = dot(qs[...], mems[d], NT)
+    st = stats[0]
+    for i in range(1, stats.shape[0]):
+        st = st + stats[i]
+    n = conv.shape[1]
+    width = n * stats.shape[0]
+    mean = st[0:1] / width
+    var = st[1:2] / width - mean * mean
+    rows = jnp.concatenate([g[0:2, :], mean, lax.rsqrt(var + EPS)], axis=0)
+    turned = jnp.concatenate([rows, rows], axis=0).T
+    x = (conv[...] - turned[:, 2:3]) * turned[:, 3:4] * chgain[...]
+    act[:, 0:n] = (x * jax.nn.sigmoid(x)).astype(BF16)
     blk = N // 4
     for j in range(4):
         r0 = j * blk
@@ -670,7 +679,7 @@
         ci = lax.broadcasted_iota(jnp.int32, (blk, N), 1)
         total, both = None, None
         for d in range(2):
-            fc = gt[r0 : r0 + blk, d : d + 1]
+            fc = turned[r0 : r0 + blk, d : d + 1]
             mask = ri >= ci if d == 0 else ri <= ci
             table = jnp.where(mask, fc + g[2 + d : 3 + d, :], -jnp.inf)
             entry = fc + runs[d]
@@ -682,24 +691,11 @@
             inv = 1.0 / jnp.maximum(jnp.abs(den), 1.0)
             w = w * inv
             total = w if total is None else total + w
-            part = dot(qb, mems[d], NT) * (ew * inv)
+            part = past[d, r0 : r0 + blk, :] * (ew * inv)
             both = part if both is None else both + part
         both = both + dot(total.astype(BF16), v[...])
-        both = both * lax.rsqrt(jnp.mean(both * both, axis=1, keepdims=True) + EPS) * gn
-        act[r0 : r0 + blk, act.shape[1] - vw :] = both.astype(BF16)
-
-
-def join_body(pos, conv, stats, gain, held, act):
-    n = conv.shape[1]
-    st = stats[0]
-    for i in range(1, stats.shape[0]):
-        st = st + stats[i]
-    width = n * stats.shape[0]
-    mean = st[0:1] / width
-    var = st[1:2] / width - mean * mean
-    mv = jnp.concatenate([mean, lax.rsqrt(var + EPS)] + [jnp.zeros_like(mean)] * 6, axis=0).T
-    x = (conv[...] - mv[:, 0:1]) * mv[:, 1:2] * gain[...]
-    act[...] = (x * jax.nn.sigmoid(x)).astype(BF16)
+        both = both * lax.rsqrt(jnp.mean(both * both, axis=1, keepdims=True) + EPS) * gain[...]
+        act[r0 : r0 + blk, n:] = both.astype(BF16)
 
 
 def out_body(pos, act, w0, w1, give, keep):
@@ -772,7 +768,6 @@
     n = conv_bias.shape[0] // C
     fits = C == R == 4 and T == 2 and heads_here == C and B % 128 == 0 and rows % 128 == 0
     fits = fits and n % 128 == 0 and kw % 128 == 0 and vw % 128 == 0 and conv_kernel.shape[0] <= 31
-    fits = fits and 2 * n <= kw
     if not fits:
         return shards_general(
             tokens,
@@ -823,12 +818,12 @@
         width = sum(w.shape[1] for w in weights) // C
         return kernel(straight_body, [((C, rows, width), BF16)], pos, *map(hbm, weights))
 
-    def cross(turn):
+    def cross(turn, place=lambda x: x):
         got = [turn[0]]
         for d in range(1, C):
             got.append(L.along_h(turn[d], d))
         shape = (C, rows, turn[0].shape[1])
-        out = kernel(stack_body, [(shape, BF16)], pos, *got)
+        out = kernel(stack_body, [(shape, BF16)], pos, *map(place, got))
         return out.reshape(wide, -1)
 
     z_a = cross(turned((key_weight, conv_value_weight, conv_gate_weight)))
@@ -844,15 +839,16 @@
     got = []
     for d in range(C):
         got.append(L.to_part(share, d))
-    z_q = cross(turned((query_weight,)))
-    z_o = cross(turned((out_conv_weight, out_cell_weight)))
+    z_q = cross(turned((query_weight,)), hbm)
+    z_o = swap(straight((out_conv_weight, out_cell_weight)), lines)
+    z_o = z_o.reshape(wide, -1)
 
     a1, a2 = flip(z_a, 1), flip(z_a, 2)
     b1, b2 = flip(z_b, 1), flip(z_b, 2)
     a3 = flip(a1, 2)
     b3 = flip(b2, 1)
     q1, q2 = flip(z_q, 1), flip(z_q, 2)
-    q3 = flip(q1, 2)
+    q3 = flip(z_q, 3)
     o1, o2 = flip(z_o, 1), flip(z_o, 2)
     o3 = flip(o1, 2)
 
@@ -860,15 +856,17 @@
     own = own.reshape(N, D // 2)
     other = L.along_tp(own, 1)
     hid = pltpu.VMEM((R, N, wide), BF16)
-    keys, values, gates, gated, msg = kernel(
+    keys, values, gates, gated, head, tail, *msg = kernel(
         state_body,
         [
             ((N, kw), BF16),
             ((N, vw), BF16),
             ((8, N), F32),
             ((N, n), BF16),
-            ((R, vw + 32, kw), BF16),
-        ],
+            ((16, n), BF16),
+            ((16, n), BF16),
+        ]
+        + [((vw + 16, kw), BF16)] * (R - 1),
         pos,
         own,
         other,
@@ -885,13 +883,19 @@
         scratch=[hid, pltpu.VMEM((gate_weight.shape[1], N), F32)],
         far=True,
     )
-    msg = swap(msg, planes)
+    up = [(l * R + i, l * R + i + 1) for l in range(C) for i in range(R - 1)]
+    before = lax.ppermute(tail, "sp", up)
+    after = lax.ppermute(head, "sp", [(b, a) for a, b in up])
+    states = []
+    for d in range(1, R):
+        states.append(L.along_q(msg[d - 1], d))
     conv, stats = kernel(
         conv_body,
         [((N, n), F32), ((C * T, 8, N), F32)],
         pos,
         hbm(gated),
-        msg,
+        before,
+        after,
         at_col(conv_kernel),
         at_col(conv_bias.reshape(1, C * n)),
         scratch=[pltpu.VMEM((N + 32, n), F32)],
@@ -902,36 +906,24 @@
         [[(l * R + p) * T + t for l in range(C) for t in range(T)] for p in range(R)],
         ("sp", "tp"),
     )
+    queries = kernel(query_body, [((N, kw), BF16)], pos, own, other, z_q, q1, q2, q3, scratch=[hid])
     act = kernel(
         cell_body,
         [((N, n + vw), BF16)],
         pos,
-        own,
-        other,
-        z_q,
-        q1,
-        q2,
-        q3,
+        queries,
         hbm(keys),
         hbm(values),
         hbm(gates),
-        msg,
+        *states,
         (hbm(start_memory), (2, 1, vw, kw), lambda p: (0, p[0], 0, 0)),
         hbm(start_norm),
         hbm(start_level),
-        hbm(cell_gain.reshape(C, vw)),
-        scratch=[hid, pltpu.VMEM((N, kw), BF16)],
-    )
-    act = kernel(
-        join_body,
-        [((N, n + vw), BF16)],
-        pos,
+        at_col(cell_gain.reshape(1, C * vw)),
         hbm(conv),
         stats,
         at_col(channel_gain.reshape(1, C * n)),
-        (act, None),
-        alias={4: 0},
-        part=[(N, n)],
+        scratch=[pltpu.VMEM((2, N, vw), F32)],
     )
     act = swap(act.reshape(C, B, n + vw), planes)
     ends = []

time: 236 us -> 240 us (1.017)
  waiting for transfers between devices: 125 us -> 106 us
  starting transfers between devices: 67.7 us -> 83.4 us
  local copies, waits for them, and re-layouts: 0.62 us -> 7.72 us
    ppermute x15 -> x12, waiting for transfers between devices: 65.5 us -> 40.1 us  [along_h(): lax.ppermute(x, 'sp', [(h * R + q, (h + d) % C * R + q) for h in range(C)...]
    all_to_all x4, waiting for transfers between devices: 2.95 us -> 15.7 us  [swap(): return lax.all_to_all(x, axes, 0, 0, axis_index_groups=groups, tiled=True)]
    ppermute x0 -> x5, starting transfers between devices: none -> 11.1 us  [the longest x3 6.53 us: along_q(): lax.ppermute(x, 'sp', [(h * R + q, h * R + (q + d) % R) for h in range(C)...]
    ppermute x12, starting transfers between devices: 14.2 us -> 22.2 us  [flip_q(): lax.ppermute(x, 'sp', [(h * R + q, h * R + (q ^ d)) for h in range(C) for...]
    unnamed x8 -> x30, local copies, waits for them, and re-layouts: 0.02 us -> 7.72 us
    ppermute x12, waiting for transfers between devices: 56.5 us -> 50.6 us  [flip_q(): lax.ppermute(x, 'sp', [(h * R + q, h * R + (q ^ d)) for h in range(C) for...]
    ppermute x15 -> x12, starting transfers between devices: 23.5 us -> 20.6 us  [along_h(): lax.ppermute(x, 'sp', [(h * R + q, (h + d) % C * R + q) for h in range(C)...]
    pallas_call x18 -> x17, Pallas kernels: 41.3 us -> 40.7 us  [kernel(): pl.pallas_call(body, out_shape=shapes if many else shapes[0], grid_spec=p...]
  transfers between devices with their start and end apart: 38 -> 40, of which waited for: 17 -> 16; matrix products, arithmetic and copies ran while one was open for 0% -> 0% of each run, Pallas kernels for 12% -> 14%
where the time goes in v1:
time: 240 us; the launch traced here: 239 us
  waiting for transfers between devices  106 us (44%)
  starting transfers between devices  83.4 us (35%)
  Pallas kernels  40.7 us (17%)
  local copies, waits for them, and re-layouts  7.72 us (3%)
    ppermute x12, waiting for transfers between devices, flip_q(): lax.ppermute(x, 'sp', [(h * R + q, h * R + (q ^ d)) for h in range(C) for...  50.6 us
    pallas_call x17, Pallas kernels, kernel(): pl.pallas_call(body, out_shape=shapes if many else shapes[0], grid_spec=p...  40.7 us
    ppermute x12, waiting for transfers between devices, along_h(): lax.ppermute(x, 'sp', [(h * R + q, (h + d) % C * R + q) for h in range(C)...  40.1 us
    ppermute x12, starting transfers between devices, flip_q(): lax.ppermute(x, 'sp', [(h * R + q, h * R + (q ^ d)) for h in range(C) for...  22.2 us
    ppermute x12, starting transfers between devices, along_h(): lax.ppermute(x, 'sp', [(h * R + q, (h + d) % C * R + q) for h in range(C)...  20.6 us
    all_to_all x4, starting transfers between devices, swap(): return lax.all_to_all(x, axes, 0, 0, axis_index_groups=groups, tiled=True)  17.7 us
    all_to_all x4, waiting for transfers between devices, swap(): return lax.all_to_all(x, axes, 0, 0, axis_index_groups=groups, tiled=True)  15.7 us
    ppermute x4, starting transfers between devices, to_part(): lax.ppermute(x, 'sp', [(s, (s % C + d) % C * R + s // C) for s in range(s...  11 us
  transfers between devices with their start and end apart: 40, of which 16 were waited for; matrix products, arithmetic and copies ran while one was open for 0% of the time, Pallas kernels for 14%

profile of v1, /device:TPU:0, one launch (start us, length us, event | category | flops | bytes accessed | tf_op | source)
XLA Modules:
  0.0 238.7 jit_solution(9345679229709961995)
XLA Ops:
  0.1 2.4 %shard_map.179 = bf16[4,128,512]{2,1,0:T(8,128)(2,1)} custom-call(s32[4]{0:T(128)S(1)} %pad_add_fusion.pos, bf16[128,2048]{1,0:T(8,128)(2,1)} %refs_0_.6), custom_call_target="tpu_custom_call" | custom-call | tf_op jit(solution)/shard_map/pallas_call | solution.py:393
  2.5 6.3 %all-to-all-start = ((bf16[4,128,512]{2,1,0:T(8,128)(2,1)}), bf16[4,128,512]{2,1,0:T(8,128)(2,1)S(1)}, u32[]{:S(2)}, u32[]{:S(2)}) async-start(bf16[4,128,512]{2,1,0:T(8,128)(2,1)} %shard_map.179), calls=%async_computation | async-start | bytes 1048576 | tf_op jit(solution)/shard_map/all_to_all | solution.py:797
  12.6 2.4 collective-permute-start.12
  14.9 2.6 %shard_map.183 = bf16[4,128,640]{2,1,0:T(8,128)(2,1)} custom-call(s32[4]{0:T(128)S(1)} %pad_add_fusion.pos, bf16[128,512]{1,0:T(8,128)(2,1)} %refs_0_.7, bf16[128,2048]{1,0:T(8,128)(2,1)} %refs_1_.5), custom_call_target="tpu_custom_call" | custom-call | tf_op jit(solution)/shard_map/pallas_call | solution.py:393
  17.5 12.4 %all-to-all-done = bf16[4,128,512]{2,1,0:T(8,128)(2,1)S(1)} async-done(((bf16[4,128,512]{2,1,0:T(8,128)(2,1)}), bf16[4,128,512]{2,1,0:T(8,128)(2,1)S(1)}, u32[]{:S(2)}, u32[]{:S(2)}) %all-to-all-start) | async-done | bytes 524320 | tf_op jit(solution)/shard_map/all_to_all | solution.py:797
  29.9 3.5 %all-to-all-start.3 = ((bf16[4,128,640]{2,1,0:T(8,128)(2,1)}), bf16[4,128,640]{2,1,0:T(8,128)(2,1)S(1)}, u32[]{:S(2)}, u32[]{:S(2)}) async-start(bf16[4,128,640]{2,1,0:T(8,128)(2,1)} %shard_map.183), calls=%async_computation.3 | async-start | bytes 1310720 | tf_op jit(solution)/shard_map/all_to_all | solution.py:797
  36.0 4.2 %collective-permute-start.1 = (bf16[144,1024]{1,0:T(8,128)(2,1)S(1)}, bf16[144,1024]{1,0:T(8,128)(2,1)S(1)}, u32[]{:S(2)}, u32[]{:S(2)}) collective-permute-start(bf16[144,1024]{1,0:T(8,128)(2,1)S(1)} %shard_map.172), channel_id=1, source_target_pairs={{0,8},{2,16},{4,24},{6,0},{8,10},{10,18},{12,26},{14,2},{16,12},{1... | collective-permute-start | bytes 884744 | tf_op jit(solution)/shard_map/ppermute | solution.py:60
  40.2 3.8 %collective-permute-start.2 = (bf16[144,1024]{1,0:T(8,128)(2,1)S(1)}, bf16[144,1024]{1,0:T(8,128)(2,1)S(1)}, u32[]{:S(2)}, u32[]{:S(2)}) collective-permute-start(bf16[144,1024]{1,0:T(8,128)(2,1)S(1)} %shard_map.172), channel_id=1, source_target_pairs={{0,16},{2,24},{4,0},{6,8},{8,18},{10,26},{12,2},{14,10},{16,20},{1... | collective-permute-start | bytes 884744 | tf_op jit(solution)/shard_map/ppermute | solution.py:60
  44.0 2.3 collective-permute-start.3
  47.2 17.3 %collective-permute-done.13.g3 = bf16[128,512]{1,0:T(8,128)(2,1)S(1)} collective-permute-done((bf16[128,512]{1,0:T(8,128)(2,1)S(1)}, bf16[128,512]{1,0:T(8,128)(2,1)S(1)}, u32[]{:S(2)}, u32[]{:S(2)}) %collective-permute-start.13) | collective-permute-done | bytes 131104 | tf_op jit(solution)/shard_map/ppermute | solution.py:38
  67.4 11.4 %collective-permute-start.15 = (bf16[512,512]{1,0:T(8,128)(2,1)S(1)}, bf16[512,512]{1,0:T(8,128)(2,1)S(1)}, u32[]{:S(2)}, u32[]{:S(2)}) collective-permute-start(bf16[512,512]{1,0:T(8,128)(2,1)S(1)} %bitcast.25), channel_id=1, source_target_pairs={{0,4},{2,6},{4,0},{6,2},{8,12},{10,14},{12,8},{14,10},{16,20},{18,... | collective-permute-start | bytes 1572872 | tf_op jit(solution)/shard_map/ppermute | solution.py:50
  81.0 4.0 %collective-permute-start.5 = (bf16[128,256]{1,0:T(8,128)(2,1)S(1)}, bf16[128,256]{1,0:T(8,128)(2,1)S(1)}, u32[]{:S(2)}, u32[]{:S(2)}) collective-permute-start(bf16[128,256]{1,0:T(8,128)(2,1)S(1)} %get-tuple-element.40), channel_id=1, source_target_pairs={{0,8},{2,10},{4,12},{6,14},{8,16},{10,18},{12,20},{14,22},{16,24},... | collective-permute-start | bytes 196616 | tf_op jit(solution)/shard_map/ppermute | solution.py:38
  88.8 4.0 %collective-permute-done.6.g2 = bf16[128,256]{1,0:T(8,128)(2,1)S(1)} collective-permute-done((bf16[128,256]{1,0:T(8,128)(2,1)S(1)}, bf16[128,256]{1,0:T(8,128)(2,1)S(1)}, u32[]{:S(2)}, u32[]{:S(2)}) %collective-permute-start.6) | collective-permute-done | bytes 65568 | tf_op jit(solution)/shard_map/ppermute | solution.py:38
  99.9 3.0 %collective-permute-done.18.b2 = bf16[512,512]{1,0:T(8,128)(2,1)} collective-permute-done((bf16[512,512]{1,0:T(8,128)(2,1)S(1)}, bf16[512,512]{1,0:T(8,128)(2,1)}, u32[]{:S(2)}, u32[]{:S(2)}) %collective-permute-start.18) | collective-permute-done | bytes 524320 | tf_op jit(solution)/shard_map/ppermute | solution.py:50
  104.4 9.5 %collective-permute-done.16.a3 = bf16[512,512]{1,0:T(8,128)(2,1)} collective-permute-done((bf16[512,512]{1,0:T(8,128)(2,1)}, bf16[512,512]{1,0:T(8,128)(2,1)}, u32[]{:S(2)}, u32[]{:S(2)}) %collective-permute-start.16) | collective-permute-done | bytes 524320 | tf_op jit(solution)/shard_map/ppermute | solution.py:50
  113.9 3.2 %collective-permute-start.8 = (bf16[512,256]{1,0:T(8,128)(2,1)S(1)}, bf16[512,256]{1,0:T(8,128)(2,1)S(1)}, u32[]{:S(2)}, u32[]{:S(2)}) collective-permute-start(bf16[512,256]{1,0:T(8,128)(2,1)S(1)} %bitcast.28), channel_id=1, source_target_pairs={{0,2},{2,0},{4,6},{6,4},{8,10},{10,8},{12,14},{14,12},{16,18},{18,... | collective-permute-start | bytes 786440 | tf_op jit(solution)/shard_map/ppermute | solution.py:50
  117.4 19.7 %collective-permute-done.19.b3 = bf16[512,512]{1,0:T(8,128)(2,1)S(1)} collective-permute-done((bf16[512,512]{1,0:T(8,128)(2,1)}, bf16[512,512]{1,0:T(8,128)(2,1)S(1)}, u32[]{:S(2)}, u32[]{:S(2)}) %collective-permute-start.19) | collective-permute-done | bytes 524320 | tf_op jit(solution)/shard_map/ppermute | solution.py:50
  140.1 7.7 %shard_map.180 = (bf16[512,256]{1,0:T(8,128)(2,1)}, bf16[512,512]{1,0:T(8,128)(2,1)}, f32[8,512]{1,0:T(8,128)}, bf16[512,128]{1,0:T(8,128)(2,1)}, bf16[16,128]{1...) custom-call(s32[4]{0:T(128)S(1)} %pad_add_fusion.pos, ...), custom_call_target="tpu_custom_call" | custom-call | tf_op jit(solution)/shard_map/pallas_call | solution.py:393
  147.9 3.3 %collective-permute-start.23 = (bf16[16,128]{1,0:T(8,128)(2,1)}, bf16[16,128]{1,0:T(8,128)(2,1)S(1)}, u32[]{:S(2)}, u32[]{:S(2)}) collective-permute-start(bf16[16,128]{1,0:T(8,128)(2,1)} %get-tuple-element.55), channel_id=1, source_target_pairs={{0,2},{2,4},{4,6},{8,10},{10,12},{12,14},{16,18},{18,20},{20,22},{... | collective-permute-start | bytes 12296 | tf_op jit(solution)/shard_map/ppermute | solution.py:887
  153.9 2.6 %collective-permute-start.20 = (bf16[528,256]{1,0:T(8,128)(2,1)}, bf16[528,256]{1,0:T(8,128)(2,1)}, u32[]{:S(2)}, u32[]{:S(2)}) collective-permute-start(bf16[528,256]{1,0:T(8,128)(2,1)} %get-tuple-element.51), channel_id=1, source_target_pairs={{0,2},{2,4},{4,6},{6,0},{8,10},{10,12},{12,14},{14,8},{16,18},{18,... | collective-permute-start | bytes 811016 | tf_op jit(solution)/shard_map/ppermute | solution.py:44
  157.6 2.9 %collective-permute-start.22 = (bf16[528,256]{1,0:T(8,128)(2,1)}, bf16[528,256]{1,0:T(8,128)(2,1)}, u32[]{:S(2)}, u32[]{:S(2)}) collective-permute-start(bf16[528,256]{1,0:T(8,128)(2,1)} %get-tuple-element.53), channel_id=1, source_target_pairs={{0,6},{2,0},{4,2},{6,4},{8,14},{10,8},{12,10},{14,12},{16,22},{18,... | collective-permute-start | bytes 811016 | tf_op jit(solution)/shard_map/ppermute | solution.py:44
  160.5 3.2 %shard_map.181 = (f32[512,128]{1,0:T(8,128)}, f32[8,8,512]{2,1,0:T(8,128)}) custom-call(s32[4]{0:T(128)S(1)} %pad_add_fusion.pos, bf16[512,128]{1,0:T(8,128)(2,1)} %get-tuple-element.54.gated, bf16[16,128]{1,0:T(8,128)(2,1)S(1)} %collective-permute-done.23.before, bf16[16,128]{1,0:T(8,128)(2,1)S(1)} %collective-permute-done.24.after, f32[31,512]{1,0:T(8,128)} %taps.1, ...), custom_call_target="tpu_custom_call" | custom-call | tf_op jit(solution)/shard_map/pallas_call | solution.py:393
  163.7 4.2 %all-to-all-start.1 = ((f32[8,8,512]{2,1,0:T(8,128)}), f32[8,8,512]{2,1,0:T(8,128)S(1)}, u32[]{:S(2)}, u32[]{:S(2)}) async-start(f32[8,8,512]{2,1,0:T(8,128)} %get-tuple-element.58), calls=%async_computation.1 | async-start | bytes 262144 | tf_op jit(solution)/shard_map/all_to_all | solution.py:797
  174.7 6.6 %shard_map.182 = bf16[512,640]{1,0:T(8,128)(2,1)} custom-call(s32[4]{0:T(128)S(1)} %pad_add_fusion.pos, bf16[512,256]{1,0:T(8,128)(2,1)S(1)} %shard_map.176.qs, bf16[512,256]{1,0:T(8,128)(2,1)} %get-tuple-element.48.k, bf16[512,512]{1,0:T(8,128)(2,1)} %get-tuple-element.49.v, f32[8,512]{1,0:T(8,128)} %get-tuple-element.50.g, ...), custom_call_target="tpu_custom_call" | custom-call | tf_op jit(solution)/shard_map/pallas_call | solution.py:393
  181.3 3.7 %all-to-all-start.2 = ((bf16[4,128,640]{2,1,0:T(8,128)(2,1)}), bf16[4,128,640]{2,1,0:T(8,128)(2,1)S(1)}, u32[]{:S(2)}, u32[]{:S(2)}) async-start(bf16[4,128,640]{2,1,0:T(8,128)(2,1)} %bitcast.13), calls=%async_computation.2 | async-start | bytes 1310720 | tf_op jit(solution)/shard_map/all_to_all | solution.py:797
  185.8 17.6 %collective-permute-done.31.w1 = bf16[512,640]{1,0:T(8,128)(2,1)} collective-permute-done((bf16[512,640]{1,0:T(8,128)(2,1)}, bf16[512,640]{1,0:T(8,128)(2,1)}, u32[]{:S(2)}, u32[]{:S(2)}) %collective-permute-start.31) | collective-permute-done | bytes 655392 | tf_op jit(solution)/shard_map/ppermute | solution.py:50
  203.3 2.9 %all-to-all-done.2.act = bf16[4,128,640]{2,1,0:T(8,128)(2,1)S(1)} async-done(((bf16[4,128,640]{2,1,0:T(8,128)(2,1)}), bf16[4,128,640]{2,1,0:T(8,128)(2,1)S(1)}, u32[]{:S(2)}, u32[]{:S(2)}) %all-to-all-start.2) | async-done | bytes 655392 | tf_op jit(solution)/shard_map/all_to_all | solution.py:797
  206.2 2.8 %shard_map.186 = (bf16[256,1024]{1,0:T(8,128)(2,1)S(1)}, f32[256,1024]{1,0:T(8,128)S(1)}) custom-call(s32[4]{0:T(128)S(1)} %pad_add_fusion.pos, bf16[4,128,640]{2,1,0:T(8,128)(2,1)S(1)} %all-to-all-done.2.act, bf16[512,640]{1,0:T(8,128)(2,1)} %collective-permute-done.30.w0, bf16[512,640]{1,0:T(8,128)(2,1)} %collective-permute-done.31.w1), custom_call_target="tpu_custom_call" | custom-call | tf_op jit(solution)/shard_map/pallas_call | solution.py:393
  209.1 2.6 %shard_map.184 = (bf16[256,1024]{1,0:T(8,128)(2,1)S(1)}, f32[256,1024]{1,0:T(8,128)S(1)}) custom-call(s32[4]{0:T(128)S(1)} %pad_add_fusion.pos, bf16[4,128,640]{2,1,0:T(8,128)(2,1)S(1)} %all-to-all-done.2.act, bf16[512,640]{1,0:T(8,128)(2,1)S(1)} %bitcast.20, bf16[512,640]{1,0:T(8,128)(2,1)} %collective-permute-done.25.w1), custom_call_target="tpu_custom_call" | custom-call | tf_op jit(solution)/shard_map/pallas_call | solution.py:393
  214.6 2.4 collective-permute-start.34
  223.0 7.8 %collective-permute-done.34.refs_6_ = bf16[64,1024]{1,0:T(8,128)(2,1)S(1)} collective-permute-done((bf16[64,1024]{1,0:T(8,128)(2,1)S(1)}, bf16[64,1024]{1,0:T(8,128)(2,1)S(1)}, u32[]{:S(2)}, u32[]{:S(2)}) %collective-permute-start.34) | collective-permute-done | bytes 131104 | tf_op jit(solution)/shard_map/ppermute | solution.py:38
  230.8 6.5 %collective-permute-done.28.refs_2_ = bf16[64,1024]{1,0:T(8,128)(2,1)S(1)} collective-permute-done((bf16[64,1024]{1,0:T(8,128)(2,1)S(1)}, bf16[64,1024]{1,0:T(8,128)(2,1)S(1)}, u32[]{:S(2)}, u32[]{:S(2)}) %collective-permute-start.28) | collective-permute-done | bytes 131104 | tf_op jit(solution)/shard_map/ppermute | solution.py:38
  (96 shorter events, 49.5 us)
Async XLA Ops:
  2.5 27.4 %all-to-all-start = ((bf16[4,128,512]{2,1,0:T(8,128)(2,1)}), bf16[4,128,512]{2,1,0:T(8,128)(2,1)S(1)}, u32[]{:S(2)}, u32[]{:S(2)}) async-start(bf16[4,128,512]{2,1,0:T(8,128)(2,1)} %shard_map.179), calls=%async_computation | async-start | bytes 1048576 | tf_op jit(solution)/shard_map/all_to_all | solution.py:797
  10.5 33.5 %collective-permute-start.11 = (bf16[128,512]{1,0:T(8,128)(2,1)S(1)}, bf16[128,512]{1,0:T(8,128)(2,1)S(1)}, u32[]{:S(2)}, u32[]{:S(2)}) collective-permute-start(bf16[128,512]{1,0:T(8,128)(2,1)S(1)} %get-tuple-element.44), channel_id=1, source_target_pairs={{0,8},{2,10},{4,12},{6,14},{8,16},{10,18},{12,20},{14,22},{16,24},... | collective-permute-start | bytes 393224 | tf_op jit(solution)/shard_map/ppermute | solution.py:38
  12.6 33.7 %collective-permute-start.12 = (bf16[128,512]{1,0:T(8,128)(2,1)S(1)}, bf16[128,512]{1,0:T(8,128)(2,1)S(1)}, u32[]{:S(2)}, u32[]{:S(2)}) collective-permute-start(bf16[128,512]{1,0:T(8,128)(2,1)S(1)} %get-tuple-element.45), channel_id=1, source_target_pairs={{0,16},{2,18},{4,20},{6,22},{8,24},{10,26},{12,28},{14,30},{16,0},... | collective-permute-start | bytes 393224 | tf_op jit(solution)/shard_map/ppermute | solution.py:38
  29.9 69.3 %all-to-all-start.3 = ((bf16[4,128,640]{2,1,0:T(8,128)(2,1)}), bf16[4,128,640]{2,1,0:T(8,128)(2,1)S(1)}, u32[]{:S(2)}, u32[]{:S(2)}) async-start(bf16[4,128,640]{2,1,0:T(8,128)(2,1)} %shard_map.183), calls=%async_computation.3 | async-start | bytes 1310720 | tf_op jit(solution)/shard_map/all_to_all | solution.py:797
  35.3 31.4 %collective-permute-start = (bf16[144,1024]{1,0:T(8,128)(2,1)S(1)}, bf16[144,1024]{1,0:T(8,128)(2,1)S(1)}, u32[]{:S(2)}, u32[]{:S(2)}) collective-permute-start(bf16[144,1024]{1,0:T(8,128)(2,1)S(1)} %shard_map.172), channel_id=1, source_target_pairs={{0,0},{2,8},{4,16},{6,24},{8,2},{10,10},{12,18},{14,26},{16,4},{18... | collective-permute-start | bytes 884744 | tf_op jit(solution)/shard_map/ppermute | solution.py:60
  36.0 30.7 %collective-permute-start.1 = (bf16[144,1024]{1,0:T(8,128)(2,1)S(1)}, bf16[144,1024]{1,0:T(8,128)(2,1)S(1)}, u32[]{:S(2)}, u32[]{:S(2)}) collective-permute-start(bf16[144,1024]{1,0:T(8,128)(2,1)S(1)} %shard_map.172), channel_id=1, source_target_pairs={{0,8},{2,16},{4,24},{6,0},{8,10},{10,18},{12,26},{14,2},{16,12},{1... | collective-permute-start | bytes 884744 | tf_op jit(solution)/shard_map/ppermute | solution.py:60
  40.2 26.4 %collective-permute-start.2 = (bf16[144,1024]{1,0:T(8,128)(2,1)S(1)}, bf16[144,1024]{1,0:T(8,128)(2,1)S(1)}, u32[]{:S(2)}, u32[]{:S(2)}) collective-permute-start(bf16[144,1024]{1,0:T(8,128)(2,1)S(1)} %shard_map.172), channel_id=1, source_target_pairs={{0,16},{2,24},{4,0},{6,8},{8,18},{10,26},{12,2},{14,10},{16,20},{1... | collective-permute-start | bytes 884744 | tf_op jit(solution)/shard_map/ppermute | solution.py:60
  44.0 22.7 %collective-permute-start.3 = (bf16[144,1024]{1,0:T(8,128)(2,1)S(1)}, bf16[144,1024]{1,0:T(8,128)(2,1)S(1)}, u32[]{:S(2)}, u32[]{:S(2)}) collective-permute-start(bf16[144,1024]{1,0:T(8,128)(2,1)S(1)} %shard_map.172), channel_id=1, source_target_pairs={{0,24},{2,0},{4,8},{6,16},{8,26},{10,2},{12,10},{14,18},{16,28},{1... | collective-permute-start | bytes 884744 | tf_op jit(solution)/shard_map/ppermute | solution.py:60
  46.3 18.2 %collective-permute-start.13 = (bf16[128,512]{1,0:T(8,128)(2,1)S(1)}, bf16[128,512]{1,0:T(8,128)(2,1)S(1)}, u32[]{:S(2)}, u32[]{:S(2)}) collective-permute-start(bf16[128,512]{1,0:T(8,128)(2,1)S(1)} %get-tuple-element.46), channel_id=1, source_target_pairs={{0,24},{2,26},{4,28},{6,30},{8,0},{10,2},{12,4},{14,6},{16,8},{18,... | collective-permute-start | bytes 393224 | tf_op jit(solution)/shard_map/ppermute | solution.py:38
  65.1 28.9 %collective-permute-start.14 = (bf16[512,512]{1,0:T(8,128)(2,1)S(1)}, bf16[512,512]{1,0:T(8,128)(2,1)}, u32[]{:S(2)}, u32[]{:S(2)}) collective-permute-start(bf16[512,512]{1,0:T(8,128)(2,1)S(1)} %bitcast.24), channel_id=1, source_target_pairs={{0,2},{2,0},{4,6},{6,4},{8,10},{10,8},{12,14},{14,12},{16,18},{18,... | collective-permute-start | bytes 1572872 | tf_op jit(solution)/shard_map/ppermute | solution.py:50
  67.3 49.8 %collective-permute-start.4 = (bf16[512,1024]{1,0:T(8,128)(2,1)S(1)}, bf16[512,1024]{1,0:T(8,128)(2,1)S(1)}, u32[]{:S(2)}, u32[]{:S(2)}) collective-permute-start(bf16[512,1024]{1,0:T(8,128)(2,1)S(1)} %bitcast.15), channel_id=1, source_target_pairs={{0,1},{1,0},{2,3},{3,2},{4,5},{5,4},{6,7},{7,6},{8,9},{9,8},{10,11... | collective-permute-start | bytes 3145736 | tf_op jit(solution)/shard_map/ppermute | solution.py:56
  67.4 31.1 %collective-permute-start.15 = (bf16[512,512]{1,0:T(8,128)(2,1)S(1)}, bf16[512,512]{1,0:T(8,128)(2,1)S(1)}, u32[]{:S(2)}, u32[]{:S(2)}) collective-permute-start(bf16[512,512]{1,0:T(8,128)(2,1)S(1)} %bitcast.25), channel_id=1, source_target_pairs={{0,4},{2,6},{4,0},{6,2},{8,12},{10,14},{12,8},{14,10},{16,20},{18,... | collective-permute-start | bytes 1572872 | tf_op jit(solution)/shard_map/ppermute | solution.py:50
  78.8 24.1 %collective-permute-start.18 = (bf16[512,512]{1,0:T(8,128)(2,1)S(1)}, bf16[512,512]{1,0:T(8,128)(2,1)}, u32[]{:S(2)}, u32[]{:S(2)}) collective-permute-start(bf16[512,512]{1,0:T(8,128)(2,1)S(1)} %bitcast.21), channel_id=1, source_target_pairs={{0,4},{2,6},{4,0},{6,2},{8,12},{10,14},{12,8},{14,10},{16,20},{18,... | collective-permute-start | bytes 1572872 | tf_op jit(solution)/shard_map/ppermute | solution.py:50
  94.0 19.9 %collective-permute-start.16 = (bf16[512,512]{1,0:T(8,128)(2,1)}, bf16[512,512]{1,0:T(8,128)(2,1)}, u32[]{:S(2)}, u32[]{:S(2)}) collective-permute-start(bf16[512,512]{1,0:T(8,128)(2,1)} %collective-permute-done.14.a1), channel_id=1, source_target_pairs={{0,4},{2,6},{4,0},{6,2},{8,12},{10,14},{12,8},{14,10},{16,20},{18,... | collective-permute-start | bytes 1572872 | tf_op jit(solution)/shard_map/ppermute | solution.py:50
  97.1 16.9 %collective-permute-start.17 = (bf16[512,512]{1,0:T(8,128)(2,1)S(1)}, bf16[512,512]{1,0:T(8,128)(2,1)}, u32[]{:S(2)}, u32[]{:S(2)}) collective-permute-start(bf16[512,512]{1,0:T(8,128)(2,1)S(1)} %bitcast.22), channel_id=1, source_target_pairs={{0,2},{2,0},{4,6},{6,4},{8,10},{10,8},{12,14},{14,12},{16,18},{18,... | collective-permute-start | bytes 1572872 | tf_op jit(solution)/shard_map/ppermute | solution.py:50
  99.3 69.8 %collective-permute-start.25 = (bf16[512,640]{1,0:T(8,128)(2,1)S(1)}, bf16[512,640]{1,0:T(8,128)(2,1)}, u32[]{:S(2)}, u32[]{:S(2)}) collective-permute-start(bf16[512,640]{1,0:T(8,128)(2,1)S(1)} %bitcast.18), channel_id=1, source_target_pairs={{0,2},{2,0},{4,6},{6,4},{8,10},{10,8},{12,14},{14,12},{16,18},{18,... | collective-permute-start | bytes 1966088 | tf_op jit(solution)/shard_map/ppermute | solution.py:50
  102.9 34.2 %collective-permute-start.19 = (bf16[512,512]{1,0:T(8,128)(2,1)}, bf16[512,512]{1,0:T(8,128)(2,1)S(1)}, u32[]{:S(2)}, u32[]{:S(2)}) collective-permute-start(bf16[512,512]{1,0:T(8,128)(2,1)} %collective-permute-done.18.b2), channel_id=1, source_target_pairs={{0,2},{2,0},{4,6},{6,4},{8,10},{10,8},{12,14},{14,12},{16,18},{18,... | collective-permute-start | bytes 1572872 | tf_op jit(solution)/shard_map/ppermute | solution.py:50
  113.9 37.3 %collective-permute-start.10 = (bf16[512,256]{1,0:T(8,128)(2,1)S(1)}, bf16[512,256]{1,0:T(8,128)(2,1)S(1)}, u32[]{:S(2)}, u32[]{:S(2)}) collective-permute-start(bf16[512,256]{1,0:T(8,128)(2,1)S(1)} %bitcast.27), channel_id=1, source_target_pairs={{0,6},{2,4},{4,2},{6,0},{8,14},{10,12},{12,10},{14,8},{16,22},{18,... | collective-permute-start | bytes 786440 | tf_op jit(solution)/shard_map/ppermute | solution.py:50
  113.9 39.3 %collective-permute-start.8 = (bf16[512,256]{1,0:T(8,128)(2,1)S(1)}, bf16[512,256]{1,0:T(8,128)(2,1)S(1)}, u32[]{:S(2)}, u32[]{:S(2)}) collective-permute-start(bf16[512,256]{1,0:T(8,128)(2,1)S(1)} %bitcast.28), channel_id=1, source_target_pairs={{0,2},{2,0},{4,6},{6,4},{8,10},{10,8},{12,14},{14,12},{16,18},{18,... | collective-permute-start | bytes 786440 | tf_op jit(solution)/shard_map/ppermute | solution.py:50
  117.1 50.8 %collective-permute-start.9 = (bf16[512,256]{1,0:T(8,128)(2,1)S(1)}, bf16[512,256]{1,0:T(8,128)(2,1)}, u32[]{:S(2)}, u32[]{:S(2)}) collective-permute-start(bf16[512,256]{1,0:T(8,128)(2,1)S(1)} %bitcast.29), channel_id=1, source_target_pairs={{0,4},{2,6},{4,0},{6,2},{8,12},{10,14},{12,8},{14,10},{16,20},{18,... | collective-permute-start | bytes 786440 | tf_op jit(solution)/shard_map/ppermute | solution.py:50
  153.9 20.8 %collective-permute-start.20 = (bf16[528,256]{1,0:T(8,128)(2,1)}, bf16[528,256]{1,0:T(8,128)(2,1)}, u32[]{:S(2)}, u32[]{:S(2)}) collective-permute-start(bf16[528,256]{1,0:T(8,128)(2,1)} %get-tuple-element.51), channel_id=1, source_target_pairs={{0,2},{2,4},{4,6},{6,0},{8,10},{10,12},{12,14},{14,8},{16,18},{18,... | collective-permute-start | bytes 811016 | tf_op jit(solution)/shard_map/ppermute | solution.py:44
  156.5 18.2 %collective-permute-start.21 = (bf16[528,256]{1,0:T(8,128)(2,1)}, bf16[528,256]{1,0:T(8,128)(2,1)}, u32[]{:S(2)}, u32[]{:S(2)}) collective-permute-start(bf16[528,256]{1,0:T(8,128)(2,1)} %get-tuple-element.52), channel_id=1, source_target_pairs={{0,4},{2,6},{4,0},{6,2},{8,12},{10,14},{12,8},{14,10},{16,20},{18,... | collective-permute-start | bytes 811016 | tf_op jit(solution)/shard_map/ppermute | solution.py:44
  157.6 17.1 %collective-permute-start.22 = (bf16[528,256]{1,0:T(8,128)(2,1)}, bf16[528,256]{1,0:T(8,128)(2,1)}, u32[]{:S(2)}, u32[]{:S(2)}) collective-permute-start(bf16[528,256]{1,0:T(8,128)(2,1)} %get-tuple-element.53), channel_id=1, source_target_pairs={{0,6},{2,0},{4,2},{6,4},{8,14},{10,8},{12,10},{14,12},{16,22},{18,... | collective-permute-start | bytes 811016 | tf_op jit(solution)/shard_map/ppermute | solution.py:44
  163.7 11.0 %all-to-all-start.1 = ((f32[8,8,512]{2,1,0:T(8,128)}), f32[8,8,512]{2,1,0:T(8,128)S(1)}, u32[]{:S(2)}, u32[]{:S(2)}) async-start(f32[8,8,512]{2,1,0:T(8,128)} %get-tuple-element.58), calls=%async_computation.1 | async-start | bytes 262144 | tf_op jit(solution)/shard_map/all_to_all | solution.py:797
  168.0 17.8 %collective-permute-start.30 = (bf16[512,640]{1,0:T(8,128)(2,1)S(1)}, bf16[512,640]{1,0:T(8,128)(2,1)}, u32[]{:S(2)}, u32[]{:S(2)}) collective-permute-start(bf16[512,640]{1,0:T(8,128)(2,1)S(1)} %bitcast.19), channel_id=1, source_target_pairs={{0,4},{2,6},{4,0},{6,2},{8,12},{10,14},{12,8},{14,10},{16,20},{18,... | collective-permute-start | bytes 1966088 | tf_op jit(solution)/shard_map/ppermute | solution.py:50
  169.1 34.2 %collective-permute-start.31 = (bf16[512,640]{1,0:T(8,128)(2,1)}, bf16[512,640]{1,0:T(8,128)(2,1)}, u32[]{:S(2)}, u32[]{:S(2)}) collective-permute-start(bf16[512,640]{1,0:T(8,128)(2,1)} %collective-permute-done.25.w1), channel_id=1, source_target_pairs={{0,4},{2,6},{4,0},{6,2},{8,12},{10,14},{12,8},{14,10},{16,20},{18,... | collective-permute-start | bytes 1966088 | tf_op jit(solution)/shard_map/ppermute | solution.py:50
  181.3 24.9 %all-to-all-start.2 = ((bf16[4,128,640]{2,1,0:T(8,128)(2,1)}), bf16[4,128,640]{2,1,0:T(8,128)(2,1)S(1)}, u32[]{:S(2)}, u32[]{:S(2)}) async-start(bf16[4,128,640]{2,1,0:T(8,128)(2,1)} %bitcast.13), calls=%async_computation.2 | async-start | bytes 1310720 | tf_op jit(solution)/shard_map/all_to_all | solution.py:797
  214.6 16.1 %collective-permute-start.34 = (bf16[64,1024]{1,0:T(8,128)(2,1)S(1)}, bf16[64,1024]{1,0:T(8,128)(2,1)S(1)}, u32[]{:S(2)}, u32[]{:S(2)}) collective-permute-start(bf16[64,1024]{1,0:T(8,128)(2,1)S(1)} %get-tuple-element.69), channel_id=1, source_target_pairs={{0,16},{2,18},{4,20},{6,22},{8,24},{10,26},{12,28},{14,30},{16,0},... | collective-permute-start | bytes 393224 | tf_op jit(solution)/shard_map/ppermute | solution.py:38
  217.0 13.7 %collective-permute-start.35 = (bf16[64,1024]{1,0:T(8,128)(2,1)S(1)}, bf16[64,1024]{1,0:T(8,128)(2,1)S(1)}, u32[]{:S(2)}, u32[]{:S(2)}) collective-permute-start(bf16[64,1024]{1,0:T(8,128)(2,1)S(1)} %get-tuple-element.70), channel_id=1, source_target_pairs={{0,24},{2,26},{4,28},{6,30},{8,0},{10,2},{12,4},{14,6},{16,8},{18,... | collective-permute-start | bytes 393224 | tf_op jit(solution)/shard_map/ppermute | solution.py:38
  219.1 11.6 %collective-permute-start.27 = (bf16[64,1024]{1,0:T(8,128)(2,1)S(1)}, bf16[64,1024]{1,0:T(8,128)(2,1)S(1)}, u32[]{:S(2)}, u32[]{:S(2)}) collective-permute-start(bf16[64,1024]{1,0:T(8,128)(2,1)S(1)} %get-tuple-element.62), channel_id=1, source_target_pairs={{0,8},{2,10},{4,12},{6,14},{8,16},{10,18},{12,20},{14,22},{16,24},... | collective-permute-start | bytes 393224 | tf_op jit(solution)/shard_map/ppermute | solution.py:38
  219.7 17.5 %collective-permute-start.28 = (bf16[64,1024]{1,0:T(8,128)(2,1)S(1)}, bf16[64,1024]{1,0:T(8,128)(2,1)S(1)}, u32[]{:S(2)}, u32[]{:S(2)}) collective-permute-start(bf16[64,1024]{1,0:T(8,128)(2,1)S(1)} %get-tuple-element.63), channel_id=1, source_target_pairs={{0,16},{2,18},{4,20},{6,22},{8,24},{10,26},{12,28},{14,30},{16,0},... | collective-permute-start | bytes 393224 | tf_op jit(solution)/shard_map/ppermute | solution.py:38
  221.3 15.9 %collective-permute-start.29 = (bf16[64,1024]{1,0:T(8,128)(2,1)S(1)}, bf16[64,1024]{1,0:T(8,128)(2,1)S(1)}, u32[]{:S(2)}, u32[]{:S(2)}) collective-permute-start(bf16[64,1024]{1,0:T(8,128)(2,1)S(1)} %get-tuple-element.64), channel_id=1, source_target_pairs={{0,24},{2,26},{4,28},{6,30},{8,0},{10,2},{12,4},{14,6},{16,8},{18,... | collective-permute-start | bytes 393224 | tf_op jit(solution)/shard_map/ppermute | solution.py:38
  (23 other events, 175.2 us)

commit v2 on v1

--- a/solution.py
+++ b/solution.py
@@ -370,7 +370,6 @@
 
 HIGHEST = lax.Precision.HIGHEST
 NT = ((1,), (1,))
-TN = ((0,), (0,))
 
 
 def kernel(body, outs, pos, *args, scratch=(), limit=24 << 20, alias=None, part=None, far=False):
@@ -555,34 +554,33 @@
     zero = jnp.zeros_like(f)
     g_out[...] = jnp.concatenate([f, b, inf - f, inb - b, zero, zero, zero, zero], axis=0)
     w8 = jnp.concatenate([wf, wb, zero, zero, zero, zero, zero, zero], axis=0)
-    wt = w8.T
     nn = None
     for t in three(w8):
         t = dot(t.astype(BF16), k)
         nn = t if nn is None else nn + t
     v = projected(pos, hid, (b0, b1, b2, b3)).astype(BF16)
     v_out[...] = v
-    v32 = v.astype(F32)
-    mf = dot((v32 * wt[:, 0:1]).astype(BF16), k, TN).astype(BF16)
-    mb = dot((v32 * wt[:, 1:2]).astype(BF16), k, TN).astype(BF16)
+    kt = k.astype(F32).T
+    mf = dot((kt * wf).astype(BF16), v).astype(BF16)
+    mb = dot((kt * wb).astype(BF16), v).astype(BF16)
 
     def small(n1, lv, ps):
+        n1 = jnp.concatenate([n1, jnp.zeros((1, v.shape[1] - n1.shape[1]), F32)], axis=1)
         wide_ = lambda x: jnp.broadcast_to(x, n1.shape)
         r = list(three(n1)) + [wide_(x) for x in three(lv)] + [wide_(x) for x in three(ps)]
         return jnp.concatenate(r + [jnp.zeros((7, n1.shape[1]), F32)], axis=0).astype(BF16)
 
     sf, sb = small(nn[0:1], lvf, pf), small(nn[1:2], lvb, pb)
-    vw = mf.shape[0]
     for d, msg in enumerate((m1, m2, m3)):
         @pl.when(q + d + 1 < R)
         def _():
-            msg[0:vw, :] = mf
-            msg[vw:, :] = sf
+            msg[0:kw, :] = mf
+            msg[kw:, :] = sf
 
         @pl.when(q + d + 1 >= R)
         def _():
-            msg[0:vw, :] = mb
-            msg[vw:, :] = sb
+            msg[0:kw, :] = mb
+            msg[kw:, :] = sb
 
 
 def conv_body(pos, gated, before, after, taps, bias, conv, stats, pad):
@@ -617,16 +615,15 @@
     pos, qs, k, v, g, m1, m2, m3, mem0, nrm0, lev0, gain, conv, stats, chgain, act, past
 ):
     h, q = pos[0], pos[1]
-    N, _ = qs.shape
-    vw = v.shape[1]
+    N, kw = qs.shape
     got = (m1, m2, m3)
     lv, ps, nr = [], [], []
     for m in got:
-        e = m[vw : vw + 16, :].astype(F32)
-        nr.append(e[0:1] + e[1:2] + e[2:3])
+        e = m[kw : kw + 16, :].astype(F32)
+        nr.append((e[0:1] + e[1:2] + e[2:3])[:, 0:kw])
         lv.append((e[3:4] + e[4:5] + e[5:6])[:, 0:1])
         ps.append((e[6:7] + e[7:8] + e[8:9])[:, 0:1])
-    mems, nrms, runs = [], [], []
+    nrms, runs = [], []
     for d in range(2):
         def ok(i):
             return q >= i + 1 if d == 0 else q < i + 1
@@ -648,16 +645,17 @@
         for y in lvs[1:]:
             run = jnp.maximum(run, y)
         ws = [jnp.exp(y - run) for y in lvs]
-        mm = ws[3] * mem0[d, 0]
+        mm = None
         nm = ws[3] * nrm0[d, pl.ds(h, 1), :]
         for i in range(3):
-            mm = mm + ws[i] * got[i][0:vw, :].astype(F32)
+            t = ws[i] * got[i][0:kw, :].astype(F32)
+            mm = t if mm is None else mm + t
             nm = nm + ws[i] * nr[i]
-        mems.append(mm.astype(BF16))
+        past[d] = dot(qs[...], mm.astype(BF16)) + dot(
+            qs[...], (ws[3] * mem0[d, 0]).astype(BF16), NT
+        )
         nrms.append(nm)
         runs.append(run)
-    for d in range(2):
-        past[d] = dot(qs[...], mems[d], NT)
     st = stats[0]
     for i in range(1, stats.shape[0]):
         st = st + stats[i]
@@ -767,7 +765,7 @@
     vw = start_memory.shape[2]
     n = conv_bias.shape[0] // C
     fits = C == R == 4 and T == 2 and heads_here == C and B % 128 == 0 and rows % 128 == 0
-    fits = fits and n % 128 == 0 and kw % 128 == 0 and vw % 128 == 0 and conv_kernel.shape[0] <= 31
+    fits = fits and kw <= vw and n % 128 == 0 and kw % 128 == 0 and vw % 128 == 0 and conv_kernel.shape[0] <= 31
     if not fits:
         return shards_general(
             tokens,
@@ -866,7 +864,7 @@
             ((16, n), BF16),
             ((16, n), BF16),
         ]
-        + [((vw + 16, kw), BF16)] * (R - 1),
+        + [((kw + 16, vw), BF16)] * (R - 1),
         pos,
         own,
         other,

time: 240 us -> 240 us (level)
  no operation moved by 1% of the time
where the time goes in v2:
time: 240 us; the launch traced here: 239 us
  waiting for transfers between devices  107 us (45%)
  starting transfers between devices  83.4 us (35%)
  Pallas kernels  40.4 us (17%)
  local copies, waits for them, and re-layouts  7.72 us (3%)
    ppermute x12, waiting for transfers between devices, flip_q(): lax.ppermute(x, 'sp', [(h * R + q, h * R + (q ^ d)) for h in range(C) for...  50.8 us
    pallas_call x17, Pallas kernels, kernel(): pl.pallas_call(body, out_shape=shapes if many else shapes[0], grid_spec=p...  40.4 us
    ppermute x12, waiting for transfers between devices, along_h(): lax.ppermute(x, 'sp', [(h * R + q, (h + d) % C * R + q) for h in range(C)...  40.1 us
    ppermute x12, starting transfers between devices, flip_q(): lax.ppermute(x, 'sp', [(h * R + q, h * R + (q ^ d)) for h in range(C) for...  22.2 us
    ppermute x12, starting transfers between devices, along_h(): lax.ppermute(x, 'sp', [(h * R + q, (h + d) % C * R + q) for h in range(C)...  20.6 us
    all_to_all x4, starting transfers between devices, swap(): return lax.all_to_all(x, axes, 0, 0, axis_index_groups=groups, tiled=True)  17.7 us
    all_to_all x4, waiting for transfers between devices, swap(): return lax.all_to_all(x, axes, 0, 0, axis_index_groups=groups, tiled=True)  15.7 us
    ppermute x4, starting transfers between devices, to_part(): lax.ppermute(x, 'sp', [(s, (s % C + d) % C * R + s // C) for s in range(s...  11 us
  transfers between devices with their start and end apart: 40, of which 16 were waited for; matrix products, arithmetic and copies ran while one was open for 0% of the time, Pallas kernels for 14%

profile of v2, /device:TPU:0, one launch (start us, length us, event | category | flops | bytes accessed | tf_op | source)
XLA Modules:
  0.0 238.6 jit_solution(17780506391872302586)
XLA Ops:
  0.1 2.4 %shard_map.179 = bf16[4,128,512]{2,1,0:T(8,128)(2,1)} custom-call(s32[4]{0:T(128)S(1)} %pad_add_fusion.pos, bf16[128,2048]{1,0:T(8,128)(2,1)} %refs_0_.6), custom_call_target="tpu_custom_call" | custom-call | tf_op jit(solution)/shard_map/pallas_call | solution.py:392
  2.5 6.3 %all-to-all-start = ((bf16[4,128,512]{2,1,0:T(8,128)(2,1)}), bf16[4,128,512]{2,1,0:T(8,128)(2,1)S(1)}, u32[]{:S(2)}, u32[]{:S(2)}) async-start(bf16[4,128,512]{2,1,0:T(8,128)(2,1)} %shard_map.179), calls=%async_computation | async-start | bytes 1048576 | tf_op jit(solution)/shard_map/all_to_all | solution.py:795
  12.6 2.4 collective-permute-start.12
  14.9 2.6 %shard_map.183 = bf16[4,128,640]{2,1,0:T(8,128)(2,1)} custom-call(s32[4]{0:T(128)S(1)} %pad_add_fusion.pos, bf16[128,512]{1,0:T(8,128)(2,1)} %refs_0_.7, bf16[128,2048]{1,0:T(8,128)(2,1)} %refs_1_.5), custom_call_target="tpu_custom_call" | custom-call | tf_op jit(solution)/shard_map/pallas_call | solution.py:392
  17.5 12.4 %all-to-all-done = bf16[4,128,512]{2,1,0:T(8,128)(2,1)S(1)} async-done(((bf16[4,128,512]{2,1,0:T(8,128)(2,1)}), bf16[4,128,512]{2,1,0:T(8,128)(2,1)S(1)}, u32[]{:S(2)}, u32[]{:S(2)}) %all-to-all-start) | async-done | bytes 524320 | tf_op jit(solution)/shard_map/all_to_all | solution.py:795
  29.9 3.5 %all-to-all-start.3 = ((bf16[4,128,640]{2,1,0:T(8,128)(2,1)}), bf16[4,128,640]{2,1,0:T(8,128)(2,1)S(1)}, u32[]{:S(2)}, u32[]{:S(2)}) async-start(bf16[4,128,640]{2,1,0:T(8,128)(2,1)} %shard_map.183), calls=%async_computation.3 | async-start | bytes 1310720 | tf_op jit(solution)/shard_map/all_to_all | solution.py:795
  36.0 4.2 %collective-permute-start.1 = (bf16[144,1024]{1,0:T(8,128)(2,1)S(1)}, bf16[144,1024]{1,0:T(8,128)(2,1)S(1)}, u32[]{:S(2)}, u32[]{:S(2)}) collective-permute-start(bf16[144,1024]{1,0:T(8,128)(2,1)S(1)} %shard_map.172), channel_id=1, source_target_pairs={{0,8},{2,16},{4,24},{6,0},{8,10},{10,18},{12,26},{14,2},{16,12},{1... | collective-permute-start | bytes 884744 | tf_op jit(solution)/shard_map/ppermute | solution.py:60
  40.2 3.8 %collective-permute-start.2 = (bf16[144,1024]{1,0:T(8,128)(2,1)S(1)}, bf16[144,1024]{1,0:T(8,128)(2,1)S(1)}, u32[]{:S(2)}, u32[]{:S(2)}) collective-permute-start(bf16[144,1024]{1,0:T(8,128)(2,1)S(1)} %shard_map.172), channel_id=1, source_target_pairs={{0,16},{2,24},{4,0},{6,8},{8,18},{10,26},{12,2},{14,10},{16,20},{1... | collective-permute-start | bytes 884744 | tf_op jit(solution)/shard_map/ppermute | solution.py:60
  44.0 2.3 collective-permute-start.3
  47.2 17.3 %collective-permute-done.13.g3 = bf16[128,512]{1,0:T(8,128)(2,1)S(1)} collective-permute-done((bf16[128,512]{1,0:T(8,128)(2,1)S(1)}, bf16[128,512]{1,0:T(8,128)(2,1)S(1)}, u32[]{:S(2)}, u32[]{:S(2)}) %collective-permute-start.13) | collective-permute-done | bytes 131104 | tf_op jit(solution)/shard_map/ppermute | solution.py:38
  67.4 11.4 %collective-permute-start.15 = (bf16[512,512]{1,0:T(8,128)(2,1)S(1)}, bf16[512,512]{1,0:T(8,128)(2,1)S(1)}, u32[]{:S(2)}, u32[]{:S(2)}) collective-permute-start(bf16[512,512]{1,0:T(8,128)(2,1)S(1)} %bitcast.25), channel_id=1, source_target_pairs={{0,4},{2,6},{4,0},{6,2},{8,12},{10,14},{12,8},{14,10},{16,20},{18,... | collective-permute-start | bytes 1572872 | tf_op jit(solution)/shard_map/ppermute | solution.py:50
  81.0 4.0 %collective-permute-start.5 = (bf16[128,256]{1,0:T(8,128)(2,1)S(1)}, bf16[128,256]{1,0:T(8,128)(2,1)S(1)}, u32[]{:S(2)}, u32[]{:S(2)}) collective-permute-start(bf16[128,256]{1,0:T(8,128)(2,1)S(1)} %get-tuple-element.40), channel_id=1, source_target_pairs={{0,8},{2,10},{4,12},{6,14},{8,16},{10,18},{12,20},{14,22},{16,24},... | collective-permute-start | bytes 196616 | tf_op jit(solution)/shard_map/ppermute | solution.py:38
  88.8 4.0 %collective-permute-done.6.g2 = bf16[128,256]{1,0:T(8,128)(2,1)S(1)} collective-permute-done((bf16[128,256]{1,0:T(8,128)(2,1)S(1)}, bf16[128,256]{1,0:T(8,128)(2,1)S(1)}, u32[]{:S(2)}, u32[]{:S(2)}) %collective-permute-start.6) | collective-permute-done | bytes 65568 | tf_op jit(solution)/shard_map/ppermute | solution.py:38
  99.9 3.0 %collective-permute-done.18.b2 = bf16[512,512]{1,0:T(8,128)(2,1)} collective-permute-done((bf16[512,512]{1,0:T(8,128)(2,1)S(1)}, bf16[512,512]{1,0:T(8,128)(2,1)}, u32[]{:S(2)}, u32[]{:S(2)}) %collective-permute-start.18) | collective-permute-done | bytes 524320 | tf_op jit(solution)/shard_map/ppermute | solution.py:50
  104.4 9.5 %collective-permute-done.16.a3 = bf16[512,512]{1,0:T(8,128)(2,1)} collective-permute-done((bf16[512,512]{1,0:T(8,128)(2,1)}, bf16[512,512]{1,0:T(8,128)(2,1)}, u32[]{:S(2)}, u32[]{:S(2)}) %collective-permute-start.16) | collective-permute-done | bytes 524320 | tf_op jit(solution)/shard_map/ppermute | solution.py:50
  113.9 3.2 %collective-permute-start.8 = (bf16[512,256]{1,0:T(8,128)(2,1)S(1)}, bf16[512,256]{1,0:T(8,128)(2,1)S(1)}, u32[]{:S(2)}, u32[]{:S(2)}) collective-permute-start(bf16[512,256]{1,0:T(8,128)(2,1)S(1)} %bitcast.28), channel_id=1, source_target_pairs={{0,2},{2,0},{4,6},{6,4},{8,10},{10,8},{12,14},{14,12},{16,18},{18,... | collective-permute-start | bytes 786440 | tf_op jit(solution)/shard_map/ppermute | solution.py:50
  117.4 19.7 %collective-permute-done.19.b3 = bf16[512,512]{1,0:T(8,128)(2,1)S(1)} collective-permute-done((bf16[512,512]{1,0:T(8,128)(2,1)}, bf16[512,512]{1,0:T(8,128)(2,1)S(1)}, u32[]{:S(2)}, u32[]{:S(2)}) %collective-permute-start.19) | collective-permute-done | bytes 524320 | tf_op jit(solution)/shard_map/ppermute | solution.py:50
  140.1 7.7 %shard_map.180 = (bf16[512,256]{1,0:T(8,128)(2,1)}, bf16[512,512]{1,0:T(8,128)(2,1)}, f32[8,512]{1,0:T(8,128)}, bf16[512,128]{1,0:T(8,128)(2,1)}, bf16[16,128]{1...) custom-call(s32[4]{0:T(128)S(1)} %pad_add_fusion.pos, ...), custom_call_target="tpu_custom_call" | custom-call | tf_op jit(solution)/shard_map/pallas_call | solution.py:392
  147.8 3.3 %collective-permute-start.23 = (bf16[16,128]{1,0:T(8,128)(2,1)}, bf16[16,128]{1,0:T(8,128)(2,1)S(1)}, u32[]{:S(2)}, u32[]{:S(2)}) collective-permute-start(bf16[16,128]{1,0:T(8,128)(2,1)} %get-tuple-element.55), channel_id=1, source_target_pairs={{0,2},{2,4},{4,6},{8,10},{10,12},{12,14},{16,18},{18,20},{20,22},{... | collective-permute-start | bytes 12296 | tf_op jit(solution)/shard_map/ppermute | solution.py:885
  153.8 2.6 %collective-permute-start.20 = (bf16[272,512]{1,0:T(8,128)(2,1)}, bf16[272,512]{1,0:T(8,128)(2,1)}, u32[]{:S(2)}, u32[]{:S(2)}) collective-permute-start(bf16[272,512]{1,0:T(8,128)(2,1)} %get-tuple-element.51), channel_id=1, source_target_pairs={{0,2},{2,4},{4,6},{6,0},{8,10},{10,12},{12,14},{14,8},{16,18},{18,... | collective-permute-start | bytes 835592 | tf_op jit(solution)/shard_map/ppermute | solution.py:44
  157.6 2.9 %collective-permute-start.22 = (bf16[272,512]{1,0:T(8,128)(2,1)}, bf16[272,512]{1,0:T(8,128)(2,1)}, u32[]{:S(2)}, u32[]{:S(2)}) collective-permute-start(bf16[272,512]{1,0:T(8,128)(2,1)} %get-tuple-element.53), channel_id=1, source_target_pairs={{0,6},{2,0},{4,2},{6,4},{8,14},{10,8},{12,10},{14,12},{16,22},{18,... | collective-permute-start | bytes 835592 | tf_op jit(solution)/shard_map/ppermute | solution.py:44
  160.4 3.2 %shard_map.181 = (f32[512,128]{1,0:T(8,128)}, f32[8,8,512]{2,1,0:T(8,128)}) custom-call(s32[4]{0:T(128)S(1)} %pad_add_fusion.pos, bf16[512,128]{1,0:T(8,128)(2,1)} %get-tuple-element.54.gated, bf16[16,128]{1,0:T(8,128)(2,1)S(1)} %collective-permute-done.23.before, bf16[16,128]{1,0:T(8,128)(2,1)S(1)} %collective-permute-done.24.after, f32[31,512]{1,0:T(8,128)} %taps.1, ...), custom_call_target="tpu_custom_call" | custom-call | tf_op jit(solution)/shard_map/pallas_call | solution.py:392
  163.7 4.2 %all-to-all-start.1 = ((f32[8,8,512]{2,1,0:T(8,128)}), f32[8,8,512]{2,1,0:T(8,128)S(1)}, u32[]{:S(2)}, u32[]{:S(2)}) async-start(f32[8,8,512]{2,1,0:T(8,128)} %get-tuple-element.58), calls=%async_computation.1 | async-start | bytes 262144 | tf_op jit(solution)/shard_map/all_to_all | solution.py:795
  174.7 6.4 %shard_map.182 = bf16[512,640]{1,0:T(8,128)(2,1)} custom-call(s32[4]{0:T(128)S(1)} %pad_add_fusion.pos, bf16[512,256]{1,0:T(8,128)(2,1)S(1)} %shard_map.176.qs, bf16[512,256]{1,0:T(8,128)(2,1)} %get-tuple-element.48.k, bf16[512,512]{1,0:T(8,128)(2,1)} %get-tuple-element.49.v, f32[8,512]{1,0:T(8,128)} %get-tuple-element.50.g, ...), custom_call_target="tpu_custom_call" | custom-call | tf_op jit(solution)/shard_map/pallas_call | solution.py:392
  181.0 3.7 %all-to-all-start.2 = ((bf16[4,128,640]{2,1,0:T(8,128)(2,1)}), bf16[4,128,640]{2,1,0:T(8,128)(2,1)S(1)}, u32[]{:S(2)}, u32[]{:S(2)}) async-start(bf16[4,128,640]{2,1,0:T(8,128)(2,1)} %bitcast.13), calls=%async_computation.2 | async-start | bytes 1310720 | tf_op jit(solution)/shard_map/all_to_all | solution.py:795
  185.7 17.6 %collective-permute-done.31.w1 = bf16[512,640]{1,0:T(8,128)(2,1)} collective-permute-done((bf16[512,640]{1,0:T(8,128)(2,1)}, bf16[512,640]{1,0:T(8,128)(2,1)}, u32[]{:S(2)}, u32[]{:S(2)}) %collective-permute-start.31) | collective-permute-done | bytes 655392 | tf_op jit(solution)/shard_map/ppermute | solution.py:50
  203.2 2.9 %all-to-all-done.2.act = bf16[4,128,640]{2,1,0:T(8,128)(2,1)S(1)} async-done(((bf16[4,128,640]{2,1,0:T(8,128)(2,1)}), bf16[4,128,640]{2,1,0:T(8,128)(2,1)S(1)}, u32[]{:S(2)}, u32[]{:S(2)}) %all-to-all-start.2) | async-done | bytes 655392 | tf_op jit(solution)/shard_map/all_to_all | solution.py:795
  206.1 2.8 %shard_map.186 = (bf16[256,1024]{1,0:T(8,128)(2,1)S(1)}, f32[256,1024]{1,0:T(8,128)S(1)}) custom-call(s32[4]{0:T(128)S(1)} %pad_add_fusion.pos, bf16[4,128,640]{2,1,0:T(8,128)(2,1)S(1)} %all-to-all-done.2.act, bf16[512,640]{1,0:T(8,128)(2,1)} %collective-permute-done.30.w0, bf16[512,640]{1,0:T(8,128)(2,1)} %collective-permute-done.31.w1), custom_call_target="tpu_custom_call" | custom-call | tf_op jit(solution)/shard_map/pallas_call | solution.py:392
  209.0 2.6 %shard_map.184 = (bf16[256,1024]{1,0:T(8,128)(2,1)S(1)}, f32[256,1024]{1,0:T(8,128)S(1)}) custom-call(s32[4]{0:T(128)S(1)} %pad_add_fusion.pos, bf16[4,128,640]{2,1,0:T(8,128)(2,1)S(1)} %all-to-all-done.2.act, bf16[512,640]{1,0:T(8,128)(2,1)S(1)} %bitcast.20, bf16[512,640]{1,0:T(8,128)(2,1)} %collective-permute-done.25.w1), custom_call_target="tpu_custom_call" | custom-call | tf_op jit(solution)/shard_map/pallas_call | solution.py:392
  214.6 2.4 collective-permute-start.34
  222.9 7.8 %collective-permute-done.34.refs_6_ = bf16[64,1024]{1,0:T(8,128)(2,1)S(1)} collective-permute-done((bf16[64,1024]{1,0:T(8,128)(2,1)S(1)}, bf16[64,1024]{1,0:T(8,128)(2,1)S(1)}, u32[]{:S(2)}, u32[]{:S(2)}) %collective-permute-start.34) | collective-permute-done | bytes 131104 | tf_op jit(solution)/shard_map/ppermute | solution.py:38
  230.7 6.5 %collective-permute-done.28.refs_2_ = bf16[64,1024]{1,0:T(8,128)(2,1)S(1)} collective-permute-done((bf16[64,1024]{1,0:T(8,128)(2,1)S(1)}, bf16[64,1024]{1,0:T(8,128)(2,1)S(1)}, u32[]{:S(2)}, u32[]{:S(2)}) %collective-permute-start.28) | collective-permute-done | bytes 131104 | tf_op jit(solution)/shard_map/ppermute | solution.py:38
  (96 shorter events, 49.8 us)
Async XLA Ops:
  2.5 27.4 %all-to-all-start = ((bf16[4,128,512]{2,1,0:T(8,128)(2,1)}), bf16[4,128,512]{2,1,0:T(8,128)(2,1)S(1)}, u32[]{:S(2)}, u32[]{:S(2)}) async-start(bf16[4,128,512]{2,1,0:T(8,128)(2,1)} %shard_map.179), calls=%async_computation | async-start | bytes 1048576 | tf_op jit(solution)/shard_map/all_to_all | solution.py:795
  10.5 33.5 %collective-permute-start.11 = (bf16[128,512]{1,0:T(8,128)(2,1)S(1)}, bf16[128,512]{1,0:T(8,128)(2,1)S(1)}, u32[]{:S(2)}, u32[]{:S(2)}) collective-permute-start(bf16[128,512]{1,0:T(8,128)(2,1)S(1)} %get-tuple-element.44), channel_id=1, source_target_pairs={{0,8},{2,10},{4,12},{6,14},{8,16},{10,18},{12,20},{14,22},{16,24},... | collective-permute-start | bytes 393224 | tf_op jit(solution)/shard_map/ppermute | solution.py:38
  12.6 33.7 %collective-permute-start.12 = (bf16[128,512]{1,0:T(8,128)(2,1)S(1)}, bf16[128,512]{1,0:T(8,128)(2,1)S(1)}, u32[]{:S(2)}, u32[]{:S(2)}) collective-permute-start(bf16[128,512]{1,0:T(8,128)(2,1)S(1)} %get-tuple-element.45), channel_id=1, source_target_pairs={{0,16},{2,18},{4,20},{6,22},{8,24},{10,26},{12,28},{14,30},{16,0},... | collective-permute-start | bytes 393224 | tf_op jit(solution)/shard_map/ppermute | solution.py:38
  29.9 69.3 %all-to-all-start.3 = ((bf16[4,128,640]{2,1,0:T(8,128)(2,1)}), bf16[4,128,640]{2,1,0:T(8,128)(2,1)S(1)}, u32[]{:S(2)}, u32[]{:S(2)}) async-start(bf16[4,128,640]{2,1,0:T(8,128)(2,1)} %shard_map.183), calls=%async_computation.3 | async-start | bytes 1310720 | tf_op jit(solution)/shard_map/all_to_all | solution.py:795
  35.3 31.4 %collective-permute-start = (bf16[144,1024]{1,0:T(8,128)(2,1)S(1)}, bf16[144,1024]{1,0:T(8,128)(2,1)S(1)}, u32[]{:S(2)}, u32[]{:S(2)}) collective-permute-start(bf16[144,1024]{1,0:T(8,128)(2,1)S(1)} %shard_map.172), channel_id=1, source_target_pairs={{0,0},{2,8},{4,16},{6,24},{8,2},{10,10},{12,18},{14,26},{16,4},{18... | collective-permute-start | bytes 884744 | tf_op jit(solution)/shard_map/ppermute | solution.py:60
  36.0 30.7 %collective-permute-start.1 = (bf16[144,1024]{1,0:T(8,128)(2,1)S(1)}, bf16[144,1024]{1,0:T(8,128)(2,1)S(1)}, u32[]{:S(2)}, u32[]{:S(2)}) collective-permute-start(bf16[144,1024]{1,0:T(8,128)(2,1)S(1)} %shard_map.172), channel_id=1, source_target_pairs={{0,8},{2,16},{4,24},{6,0},{8,10},{10,18},{12,26},{14,2},{16,12},{1... | collective-permute-start | bytes 884744 | tf_op jit(solution)/shard_map/ppermute | solution.py:60
  40.2 26.4 %collective-permute-start.2 = (bf16[144,1024]{1,0:T(8,128)(2,1)S(1)}, bf16[144,1024]{1,0:T(8,128)(2,1)S(1)}, u32[]{:S(2)}, u32[]{:S(2)}) collective-permute-start(bf16[144,1024]{1,0:T(8,128)(2,1)S(1)} %shard_map.172), channel_id=1, source_target_pairs={{0,16},{2,24},{4,0},{6,8},{8,18},{10,26},{12,2},{14,10},{16,20},{1... | collective-permute-start | bytes 884744 | tf_op jit(solution)/shard_map/ppermute | solution.py:60
  44.0 22.7 %collective-permute-start.3 = (bf16[144,1024]{1,0:T(8,128)(2,1)S(1)}, bf16[144,1024]{1,0:T(8,128)(2,1)S(1)}, u32[]{:S(2)}, u32[]{:S(2)}) collective-permute-start(bf16[144,1024]{1,0:T(8,128)(2,1)S(1)} %shard_map.172), channel_id=1, source_target_pairs={{0,24},{2,0},{4,8},{6,16},{8,26},{10,2},{12,10},{14,18},{16,28},{1... | collective-permute-start | bytes 884744 | tf_op jit(solution)/shard_map/ppermute | solution.py:60
  46.3 18.2 %collective-permute-start.13 = (bf16[128,512]{1,0:T(8,128)(2,1)S(1)}, bf16[128,512]{1,0:T(8,128)(2,1)S(1)}, u32[]{:S(2)}, u32[]{:S(2)}) collective-permute-start(bf16[128,512]{1,0:T(8,128)(2,1)S(1)} %get-tuple-element.46), channel_id=1, source_target_pairs={{0,24},{2,26},{4,28},{6,30},{8,0},{10,2},{12,4},{14,6},{16,8},{18,... | collective-permute-start | bytes 393224 | tf_op jit(solution)/shard_map/ppermute | solution.py:38
  65.1 28.9 %collective-permute-start.14 = (bf16[512,512]{1,0:T(8,128)(2,1)S(1)}, bf16[512,512]{1,0:T(8,128)(2,1)}, u32[]{:S(2)}, u32[]{:S(2)}) collective-permute-start(bf16[512,512]{1,0:T(8,128)(2,1)S(1)} %bitcast.24), channel_id=1, source_target_pairs={{0,2},{2,0},{4,6},{6,4},{8,10},{10,8},{12,14},{14,12},{16,18},{18,... | collective-permute-start | bytes 1572872 | tf_op jit(solution)/shard_map/ppermute | solution.py:50
  67.3 49.8 %collective-permute-start.4 = (bf16[512,1024]{1,0:T(8,128)(2,1)S(1)}, bf16[512,1024]{1,0:T(8,128)(2,1)S(1)}, u32[]{:S(2)}, u32[]{:S(2)}) collective-permute-start(bf16[512,1024]{1,0:T(8,128)(2,1)S(1)} %bitcast.15), channel_id=1, source_target_pairs={{0,1},{1,0},{2,3},{3,2},{4,5},{5,4},{6,7},{7,6},{8,9},{9,8},{10,11... | collective-permute-start | bytes 3145736 | tf_op jit(solution)/shard_map/ppermute | solution.py:56
  67.4 31.1 %collective-permute-start.15 = (bf16[512,512]{1,0:T(8,128)(2,1)S(1)}, bf16[512,512]{1,0:T(8,128)(2,1)S(1)}, u32[]{:S(2)}, u32[]{:S(2)}) collective-permute-start(bf16[512,512]{1,0:T(8,128)(2,1)S(1)} %bitcast.25), channel_id=1, source_target_pairs={{0,4},{2,6},{4,0},{6,2},{8,12},{10,14},{12,8},{14,10},{16,20},{18,... | collective-permute-start | bytes 1572872 | tf_op jit(solution)/shard_map/ppermute | solution.py:50
  78.8 24.1 %collective-permute-start.18 = (bf16[512,512]{1,0:T(8,128)(2,1)S(1)}, bf16[512,512]{1,0:T(8,128)(2,1)}, u32[]{:S(2)}, u32[]{:S(2)}) collective-permute-start(bf16[512,512]{1,0:T(8,128)(2,1)S(1)} %bitcast.21), channel_id=1, source_target_pairs={{0,4},{2,6},{4,0},{6,2},{8,12},{10,14},{12,8},{14,10},{16,20},{18,... | collective-permute-start | bytes 1572872 | tf_op jit(solution)/shard_map/ppermute | solution.py:50
  94.0 19.9 %collective-permute-start.16 = (bf16[512,512]{1,0:T(8,128)(2,1)}, bf16[512,512]{1,0:T(8,128)(2,1)}, u32[]{:S(2)}, u32[]{:S(2)}) collective-permute-start(bf16[512,512]{1,0:T(8,128)(2,1)} %collective-permute-done.14.a1), channel_id=1, source_target_pairs={{0,4},{2,6},{4,0},{6,2},{8,12},{10,14},{12,8},{14,10},{16,20},{18,... | collective-permute-start | bytes 1572872 | tf_op jit(solution)/shard_map/ppermute | solution.py:50
  97.1 16.9 %collective-permute-start.17 = (bf16[512,512]{1,0:T(8,128)(2,1)S(1)}, bf16[512,512]{1,0:T(8,128)(2,1)}, u32[]{:S(2)}, u32[]{:S(2)}) collective-permute-start(bf16[512,512]{1,0:T(8,128)(2,1)S(1)} %bitcast.22), channel_id=1, source_target_pairs={{0,2},{2,0},{4,6},{6,4},{8,10},{10,8},{12,14},{14,12},{16,18},{18,... | collective-permute-start | bytes 1572872 | tf_op jit(solution)/shard_map/ppermute | solution.py:50
  99.3 69.7 %collective-permute-start.25 = (bf16[512,640]{1,0:T(8,128)(2,1)S(1)}, bf16[512,640]{1,0:T(8,128)(2,1)}, u32[]{:S(2)}, u32[]{:S(2)}) collective-permute-start(bf16[512,640]{1,0:T(8,128)(2,1)S(1)} %bitcast.18), channel_id=1, source_target_pairs={{0,2},{2,0},{4,6},{6,4},{8,10},{10,8},{12,14},{14,12},{16,18},{18,... | collective-permute-start | bytes 1966088 | tf_op jit(solution)/shard_map/ppermute | solution.py:50
  102.9 34.2 %collective-permute-start.19 = (bf16[512,512]{1,0:T(8,128)(2,1)}, bf16[512,512]{1,0:T(8,128)(2,1)S(1)}, u32[]{:S(2)}, u32[]{:S(2)}) collective-permute-start(bf16[512,512]{1,0:T(8,128)(2,1)} %collective-permute-done.18.b2), channel_id=1, source_target_pairs={{0,2},{2,0},{4,6},{6,4},{8,10},{10,8},{12,14},{14,12},{16,18},{18,... | collective-permute-start | bytes 1572872 | tf_op jit(solution)/shard_map/ppermute | solution.py:50
  113.9 37.2 %collective-permute-start.10 = (bf16[512,256]{1,0:T(8,128)(2,1)S(1)}, bf16[512,256]{1,0:T(8,128)(2,1)S(1)}, u32[]{:S(2)}, u32[]{:S(2)}) collective-permute-start(bf16[512,256]{1,0:T(8,128)(2,1)S(1)} %bitcast.27), channel_id=1, source_target_pairs={{0,6},{2,4},{4,2},{6,0},{8,14},{10,12},{12,10},{14,8},{16,22},{18,... | collective-permute-start | bytes 786440 | tf_op jit(solution)/shard_map/ppermute | solution.py:50
  113.9 39.2 %collective-permute-start.8 = (bf16[512,256]{1,0:T(8,128)(2,1)S(1)}, bf16[512,256]{1,0:T(8,128)(2,1)S(1)}, u32[]{:S(2)}, u32[]{:S(2)}) collective-permute-start(bf16[512,256]{1,0:T(8,128)(2,1)S(1)} %bitcast.28), channel_id=1, source_target_pairs={{0,2},{2,0},{4,6},{6,4},{8,10},{10,8},{12,14},{14,12},{16,18},{18,... | collective-permute-start | bytes 786440 | tf_op jit(solution)/shard_map/ppermute | solution.py:50
  117.1 50.8 %collective-permute-start.9 = (bf16[512,256]{1,0:T(8,128)(2,1)S(1)}, bf16[512,256]{1,0:T(8,128)(2,1)}, u32[]{:S(2)}, u32[]{:S(2)}) collective-permute-start(bf16[512,256]{1,0:T(8,128)(2,1)S(1)} %bitcast.29), channel_id=1, source_target_pairs={{0,4},{2,6},{4,0},{6,2},{8,12},{10,14},{12,8},{14,10},{16,20},{18,... | collective-permute-start | bytes 786440 | tf_op jit(solution)/shard_map/ppermute | solution.py:50
  153.8 20.8 %collective-permute-start.20 = (bf16[272,512]{1,0:T(8,128)(2,1)}, bf16[272,512]{1,0:T(8,128)(2,1)}, u32[]{:S(2)}, u32[]{:S(2)}) collective-permute-start(bf16[272,512]{1,0:T(8,128)(2,1)} %get-tuple-element.51), channel_id=1, source_target_pairs={{0,2},{2,4},{4,6},{6,0},{8,10},{10,12},{12,14},{14,8},{16,18},{18,... | collective-permute-start | bytes 835592 | tf_op jit(solution)/shard_map/ppermute | solution.py:44
  156.5 18.2 %collective-permute-start.21 = (bf16[272,512]{1,0:T(8,128)(2,1)}, bf16[272,512]{1,0:T(8,128)(2,1)}, u32[]{:S(2)}, u32[]{:S(2)}) collective-permute-start(bf16[272,512]{1,0:T(8,128)(2,1)} %get-tuple-element.52), channel_id=1, source_target_pairs={{0,4},{2,6},{4,0},{6,2},{8,12},{10,14},{12,8},{14,10},{16,20},{18,... | collective-permute-start | bytes 835592 | tf_op jit(solution)/shard_map/ppermute | solution.py:44
  157.6 17.1 %collective-permute-start.22 = (bf16[272,512]{1,0:T(8,128)(2,1)}, bf16[272,512]{1,0:T(8,128)(2,1)}, u32[]{:S(2)}, u32[]{:S(2)}) collective-permute-start(bf16[272,512]{1,0:T(8,128)(2,1)} %get-tuple-element.53), channel_id=1, source_target_pairs={{0,6},{2,0},{4,2},{6,4},{8,14},{10,8},{12,10},{14,12},{16,22},{18,... | collective-permute-start | bytes 835592 | tf_op jit(solution)/shard_map/ppermute | solution.py:44
  163.7 11.0 %all-to-all-start.1 = ((f32[8,8,512]{2,1,0:T(8,128)}), f32[8,8,512]{2,1,0:T(8,128)S(1)}, u32[]{:S(2)}, u32[]{:S(2)}) async-start(f32[8,8,512]{2,1,0:T(8,128)} %get-tuple-element.58), calls=%async_computation.1 | async-start | bytes 262144 | tf_op jit(solution)/shard_map/all_to_all | solution.py:795
  167.9 17.8 %collective-permute-start.30 = (bf16[512,640]{1,0:T(8,128)(2,1)S(1)}, bf16[512,640]{1,0:T(8,128)(2,1)}, u32[]{:S(2)}, u32[]{:S(2)}) collective-permute-start(bf16[512,640]{1,0:T(8,128)(2,1)S(1)} %bitcast.19), channel_id=1, source_target_pairs={{0,4},{2,6},{4,0},{6,2},{8,12},{10,14},{12,8},{14,10},{16,20},{18,... | collective-permute-start | bytes 1966088 | tf_op jit(solution)/shard_map/ppermute | solution.py:50
  169.0 34.2 %collective-permute-start.31 = (bf16[512,640]{1,0:T(8,128)(2,1)}, bf16[512,640]{1,0:T(8,128)(2,1)}, u32[]{:S(2)}, u32[]{:S(2)}) collective-permute-start(bf16[512,640]{1,0:T(8,128)(2,1)} %collective-permute-done.25.w1), channel_id=1, source_target_pairs={{0,4},{2,6},{4,0},{6,2},{8,12},{10,14},{12,8},{14,10},{16,20},{18,... | collective-permute-start | bytes 1966088 | tf_op jit(solution)/shard_map/ppermute | solution.py:50
  181.0 25.1 %all-to-all-start.2 = ((bf16[4,128,640]{2,1,0:T(8,128)(2,1)}), bf16[4,128,640]{2,1,0:T(8,128)(2,1)S(1)}, u32[]{:S(2)}, u32[]{:S(2)}) async-start(bf16[4,128,640]{2,1,0:T(8,128)(2,1)} %bitcast.13), calls=%async_computation.2 | async-start | bytes 1310720 | tf_op jit(solution)/shard_map/all_to_all | solution.py:795
  214.6 16.1 %collective-permute-start.34 = (bf16[64,1024]{1,0:T(8,128)(2,1)S(1)}, bf16[64,1024]{1,0:T(8,128)(2,1)S(1)}, u32[]{:S(2)}, u32[]{:S(2)}) collective-permute-start(bf16[64,1024]{1,0:T(8,128)(2,1)S(1)} %get-tuple-element.69), channel_id=1, source_target_pairs={{0,16},{2,18},{4,20},{6,22},{8,24},{10,26},{12,28},{14,30},{16,0},... | collective-permute-start | bytes 393224 | tf_op jit(solution)/shard_map/ppermute | solution.py:38
  216.9 13.7 %collective-permute-start.35 = (bf16[64,1024]{1,0:T(8,128)(2,1)S(1)}, bf16[64,1024]{1,0:T(8,128)(2,1)S(1)}, u32[]{:S(2)}, u32[]{:S(2)}) collective-permute-start(bf16[64,1024]{1,0:T(8,128)(2,1)S(1)} %get-tuple-element.70), channel_id=1, source_target_pairs={{0,24},{2,26},{4,28},{6,30},{8,0},{10,2},{12,4},{14,6},{16,8},{18,... | collective-permute-start | bytes 393224 | tf_op jit(solution)/shard_map/ppermute | solution.py:38
  219.1 11.6 %collective-permute-start.27 = (bf16[64,1024]{1,0:T(8,128)(2,1)S(1)}, bf16[64,1024]{1,0:T(8,128)(2,1)S(1)}, u32[]{:S(2)}, u32[]{:S(2)}) collective-permute-start(bf16[64,1024]{1,0:T(8,128)(2,1)S(1)} %get-tuple-element.62), channel_id=1, source_target_pairs={{0,8},{2,10},{4,12},{6,14},{8,16},{10,18},{12,20},{14,22},{16,24},... | collective-permute-start | bytes 393224 | tf_op jit(solution)/shard_map/ppermute | solution.py:38
  219.7 17.5 %collective-permute-start.28 = (bf16[64,1024]{1,0:T(8,128)(2,1)S(1)}, bf16[64,1024]{1,0:T(8,128)(2,1)S(1)}, u32[]{:S(2)}, u32[]{:S(2)}) collective-permute-start(bf16[64,1024]{1,0:T(8,128)(2,1)S(1)} %get-tuple-element.63), channel_id=1, source_target_pairs={{0,16},{2,18},{4,20},{6,22},{8,24},{10,26},{12,28},{14,30},{16,0},... | collective-permute-start | bytes 393224 | tf_op jit(solution)/shard_map/ppermute | solution.py:38
  221.2 15.9 %collective-permute-start.29 = (bf16[64,1024]{1,0:T(8,128)(2,1)S(1)}, bf16[64,1024]{1,0:T(8,128)(2,1)S(1)}, u32[]{:S(2)}, u32[]{:S(2)}) collective-permute-start(bf16[64,1024]{1,0:T(8,128)(2,1)S(1)} %get-tuple-element.64), channel_id=1, source_target_pairs={{0,24},{2,26},{4,28},{6,30},{8,0},{10,2},{12,4},{14,6},{16,8},{18,... | collective-permute-start | bytes 393224 | tf_op jit(solution)/shard_map/ppermute | solution.py:38
  (23 other events, 175.2 us)
